TPU v7x, 512 devices: a whole 4x8x8 slice. The times are simulated.
512 devices in a mesh: sp: 32 (over z, x), tp: 16 (over y, core).
Axes of the slice: x: 4, y: 8, z: 8, core: 2. Of those that a mesh axis runs over, the one named last changes fastest.
Arguments:
- lane_source_signal: bfloat16 [1024, 4096], P('tp', 'sp'), may hold values from -6 to 6
- spectral_damping_part: float32 [64, 64], P('tp'), may hold values from -3 to -0.0002
- spectral_angular_part: float32 [64, 64], P('tp'), may hold values from 0.31 to 201.0624
- interval_exponent: float32 [64], P('tp'), may hold values from -3.9 to -1.6
- entry_matrix_inphase: float32 [64, 64, 16], P('tp'), may hold values from -1 to 1
- entry_matrix_quadrature: float32 [64, 64, 16], P('tp'), may hold values from -1 to 1
- emission_inphase: float32 [64, 16, 64], P('tp'), may hold values from -0.75 to 0.75
- emission_quadrature: float32 [64, 16, 64], P('tp'), may hold values from -0.75 to 0.75
- lane_bypass_factor: float32 [1024], P('tp'), may hold values from -5 to 5
- spike_shrink_offset: float32 [64, 4096], P('tp', 'sp'), may hold values from -1.4 to 0
- lane_exit_matrix: bfloat16 [1024, 4096], P('tp'), may hold values from -0.1875 to 0.1875
- skipline_stream: bfloat16 [4096, 4096], P('sp'), may hold values from -6 to 6
- specialist_scaling_vector: float32 [4096], replicated, may hold values from 0.1 to 1.9
- selected_specialists: int32 [4096, 2], P('sp'), may hold values from 0 to 31, all different within a row; in each aligned block of 128 rows (0 to 127, 128 to 255, ...) at most 16 rows name the same one
- dispatcher_scores: float32 [4096, 2], P('sp'), may hold values from 0.1 to 1
- specialist_valve_matrix: bfloat16 [32, 4096, 2048], P('sp', None, 'tp'), may hold values from -0.09375 to 0.09375
- specialist_widen_matrix: bfloat16 [32, 4096, 2048], P('sp', None, 'tp'), may hold values from -0.09375 to 0.09375
- specialist_shrink_matrix: bfloat16 [32, 2048, 4096], P('sp', 'tp'), may hold values from -0.1875 to 0.1875
Outputs:
- updated: bfloat16 [4096, 4096], P('sp', 'tp')
Inputs may be any that keep to these rules, and one draw needn't show every extreme that they name: `selected_specialists`: each row names 2 different experts. Among the rows of each aligned block of 128 positions no expert is named more than 16 times, and in every block some expert is named exactly 16 times.
All inputs are finite; a program needn't handle non-finite values.
Results may differ from a plain program's by a relative error of at most 0.019.
Values may be sent and summed in bfloat16 or wider, within the bound.
A program may use at most 64 MiB of HBM per device.

v0:
```python
import jax
import jax.numpy as jnp
from jax import lax
from jax.sharding import PartitionSpec as P

EPS = 1e-06
PRECISE_MODE = lax.Precision.HIGHEST


def copy_for_each(array, axis):
    copies = jnp.broadcast_to(array, (lax.axis_size(axis), *array.shape))
    return lax.all_to_all(copies, axis, split_axis=0, concat_axis=0, tiled=True)


def gathered_once(array, axis):
    leaves = jax.tree.leaves(array)
    order = sorted(range(len(leaves)), key=lambda k: -leaves[k].size)
    width = (1, *leaves[order[0]].shape)[-1]
    lines = [
        jnp.pad(leaves[k].reshape(-1), (0, -leaves[k].size % width)).reshape(-1, width)
        for k in order
    ]
    both, at, found = (copy_for_each(jnp.concatenate(lines), axis), 0, {})
    for k, line in zip(order, lines):
        share = both[:, at : at + len(line)].reshape(len(both), -1)
        found[k] = share[:, : leaves[k].size].reshape(-1, *leaves[k].shape)
        at += len(line)
    numbers = iter(range(len(leaves)))
    return jax.tree.map(lambda _: found[next(numbers)], array)


def combined_pairwise(pieces, combine):
    while len(jax.tree.leaves(pieces)[0]) > 1:
        pieces = jax.vmap(combine)(
            *(jax.tree.map(lambda part: part[side::2], pieces) for side in (0, 1))
        )
    return jax.tree.map(lambda part: part[0], pieces)


def prefix(array, axis, combine, identity):
    length, mine = (lax.axis_size(axis), lax.axis_index(axis))
    passed = jnp.arange(length) < mine

    def kept(part, zero, own):
        part = jnp.where(
            passed.reshape(-1, *(1 for _ in own.shape)), part, jnp.asarray(zero, own.dtype)
        )
        return part

    pieces = gathered_once(array, axis)
    return combined_pairwise(jax.tree.map(kept, pieces, identity, array), combine)


def in_blocks(array, dim, length):
    before, after = (array.shape[:dim], array.shape[dim + 1 :])
    return jnp.moveaxis(array.reshape(*before, length, -1, *after), dim, 0)


def sent_and_summed(array, axis, dim):
    length = lax.axis_size(axis)
    parts = lax.all_to_all(in_blocks(array, dim, length), axis, 0, 0, tiled=True)
    return jnp.sum(parts.astype(jnp.float32), axis=0)


def taken_together(array, axis):
    return copy_for_each(array, axis).sum(axis=0)


def affine_pair(earlier, latter):
    mul_re = earlier[0] * latter[0] - earlier[1] * latter[1]
    mul_im = earlier[0] * latter[1] + earlier[1] * latter[0]
    add_re = latter[0] * earlier[2] - latter[1] * earlier[3] + latter[2]
    add_im = latter[0] * earlier[3] + latter[1] * earlier[2] + latter[3]
    return (mul_re, mul_im, add_re, add_im)


def local_prefix(elements):
    length = elements[0].shape[2]
    fills = (1.0, 0.0, 0.0, 0.0)
    offset = 1
    while offset < length:
        earlier = tuple(
            (
                jnp.pad(
                    item[:, :, : length - offset],
                    ((0, 0), (0, 0), (offset, 0)),
                    constant_values=fill,
                )
                for item, fill in zip(elements, fills)
            )
        )
        elements = affine_pair(earlier, elements)
        offset = offset * 2
    return elements


def per_device(
    lane_source_signal,
    spectral_damping_part,
    spectral_angular_part,
    interval_exponent,
    entry_matrix_inphase,
    entry_matrix_quadrature,
    emission_inphase,
    emission_quadrature,
    lane_bypass_factor,
    spike_shrink_offset,
    lane_exit_matrix,
    skipline_stream,
    specialist_scaling_vector,
    selected_specialists,
    dispatcher_scores,
    specialist_valve_matrix,
    specialist_widen_matrix,
    specialist_shrink_matrix,
):
    f32 = jnp.float32
    bf16 = jnp.bfloat16
    groups_here = spectral_damping_part.shape[0]
    lanes_within_bundle = entry_matrix_inphase.shape[2]
    tok_local = lane_source_signal.shape[1]
    bundled_signal = lane_source_signal.astype(f32).reshape(
        groups_here, lanes_within_bundle, tok_local
    )
    step_size = jnp.exp(interval_exponent)[:, None]
    natural_pace_exponent = spectral_damping_part * step_size
    angle = spectral_angular_part * step_size
    num_re = jnp.expm1(natural_pace_exponent) * jnp.cos(angle) - 2.0 * jnp.sin(0.5 * angle) ** 2
    num_im = jnp.exp(natural_pace_exponent) * jnp.sin(angle)
    denom = (
        spectral_damping_part * spectral_damping_part
        + spectral_angular_part * spectral_angular_part
    )
    fac_re = (num_re * spectral_damping_part + num_im * spectral_angular_part) / denom
    fac_im = (num_im * spectral_damping_part - num_re * spectral_angular_part) / denom
    map_re = (
        fac_re[:, :, None] * entry_matrix_inphase - fac_im[:, :, None] * entry_matrix_quadrature
    )
    map_im = (
        fac_re[:, :, None] * entry_matrix_quadrature + fac_im[:, :, None] * entry_matrix_inphase
    )
    drive_re = jnp.einsum("gpc,gct->gpt", map_re, bundled_signal, precision=PRECISE_MODE)
    drive_im = jnp.einsum("gpc,gct->gpt", map_im, bundled_signal, precision=PRECISE_MODE)
    recurrence_modulus = jnp.exp(
        natural_pace_exponent[:, :, None] + spike_shrink_offset[:, None, :]
    )
    trans_re = recurrence_modulus * jnp.cos(angle)[:, :, None]
    trans_im = recurrence_modulus * jnp.sin(angle)[:, :, None]
    cum_re, cum_im, state_real, state_imaginary = local_prefix(
        (trans_re, trans_im, drive_re, drive_im)
    )
    summary = (cum_re[:, :, -1], cum_im[:, :, -1], state_real[:, :, -1], state_imaginary[:, :, -1])
    unit = jnp.ones_like(summary[0])
    blank = jnp.zeros_like(summary[0])
    carried = prefix(summary, "sp", affine_pair, (unit, blank, blank, blank))
    enter_re = carried[2][:, :, None]
    enter_im = carried[3][:, :, None]
    state_real = state_real + cum_re * enter_re - cum_im * enter_im
    state_imaginary = state_imaginary + cum_re * enter_im + cum_im * enter_re
    value = (
        jnp.einsum("nef,nfi->nei", emission_inphase, state_real, precision=PRECISE_MODE)
        - jnp.einsum("nef,nfi->nei", emission_quadrature, state_imaginary, precision=PRECISE_MODE)
        + lane_bypass_factor.reshape(groups_here, lanes_within_bundle)[:, :, None] * bundled_signal
    )
    recurrence_result = (
        jax.nn.gelu(value).astype(bf16).reshape(groups_here * lanes_within_bundle, tok_local)
    )
    width = specialist_scaling_vector.shape[0]
    d_local = width // lax.axis_size("tp")
    col_start = lax.axis_index("tp") * d_local
    partial_rows = jnp.einsum(
        "ct,cd->td", recurrence_result, lane_exit_matrix, preferred_element_type=f32
    )
    projected_own = sent_and_summed(partial_rows.astype(jnp.bfloat16), "tp", 1).astype(bf16)
    own_residual = lax.dynamic_slice_in_dim(skipline_stream, col_start, d_local, 1)
    stream_own = (
        own_residual.astype(f32) + lax.optimization_barrier(projected_own).astype(f32)
    ).astype(bf16)
    own_stream = lax.optimization_barrier(stream_own).astype(f32)
    square_total = taken_together(jnp.sum(own_stream * own_stream, axis=1), "tp")
    inv_rms = lax.rsqrt(square_total / width + EPS)[:, None]
    own_gain = lax.dynamic_slice_in_dim(specialist_scaling_vector, col_start, d_local, 0)
    own_cols = (own_stream * inv_rms * own_gain).astype(bf16)
    share = dispatcher_scores / jnp.sum(dispatcher_scores, axis=1, keepdims=True)
    experts = lax.axis_size("sp")
    top = selected_specialists.shape[1]
    capacity = 2 * tok_local * top // experts
    flat_routes = selected_specialists.reshape(-1)
    hits = (flat_routes[:, None] == jnp.arange(experts, dtype=jnp.int32)[None, :]).astype(jnp.int32)
    ranks = jnp.sum((jnp.cumsum(hits, axis=0) - hits) * hits, axis=1)
    slot_ids = flat_routes * capacity + ranks
    slot_grid = jnp.arange(experts * capacity, dtype=jnp.int32)
    matched = slot_grid[:, None] == slot_ids[None, :]
    token_of = jnp.arange(tok_local * top, dtype=jnp.int32) // top
    slot_token = jnp.sum(jnp.where(matched, token_of[None, :], 0), axis=1)
    slot_live = jnp.any(matched, axis=1)
    gate_w = specialist_valve_matrix[0]
    up_w = specialist_widen_matrix[0]
    down_w = specialist_shrink_matrix[0]
    bf_zero = jnp.zeros((), bf16)
    dispatch = jnp.where(slot_live[:, None], own_cols[slot_token], bf_zero).reshape(
        experts, capacity, d_local
    )
    arrived = lax.all_to_all(dispatch, "sp", split_axis=0, concat_axis=0, tiled=True)
    piece = lax.all_gather(arrived, "tp", axis=2, tiled=True)
    gate_part = jnp.einsum("snd,df->snf", piece, gate_w, preferred_element_type=f32)
    up_part = jnp.einsum("snd,df->snf", piece, up_w, preferred_element_type=f32)
    hidden = (jax.nn.silu(gate_part) * up_part).astype(bf16)
    flat_hidden = hidden.reshape(experts * capacity, hidden.shape[2])
    down_part = jnp.dot(flat_hidden, down_w, preferred_element_type=f32).astype(bf16)
    summed = lax.psum_scatter(
        down_part.astype(f32).astype(jnp.bfloat16), "tp", scatter_dimension=1, tiled=True
    ).astype(jnp.float32)
    expert_out = summed.astype(bf16).reshape(experts, capacity, d_local)
    returned = lax.all_to_all(expert_out, "sp", split_axis=0, concat_axis=0, tiled=True).reshape(
        experts * capacity, d_local
    )
    picked = returned[slot_ids].reshape(tok_local, top, d_local)
    combined = jnp.sum(lax.optimization_barrier(picked).astype(f32) * share[:, :, None], axis=1)
    return (own_stream + combined).astype(bf16)


def solution(mesh):
    placed = (
        P("tp", "sp"),
        P("tp", None),
        P("tp", None),
        P("tp"),
        P("tp", None, None),
        P("tp", None, None),
        P("tp", None, None),
        P("tp", None, None),
        P("tp"),
        P("tp", "sp"),
        P("tp", None),
        P("sp", None),
        P(),
        P("sp", None),
        P("sp", None),
        P("sp", None, "tp"),
        P("sp", None, "tp"),
        P("sp", "tp", None),
    )
    return jax.shard_map(
        per_device, mesh=mesh, in_specs=placed, out_specs=P("sp", "tp"), check_vma=False
    )
```

profile of v0, /device:TPU:1, one launch (start us, length us, event | category | flops | bytes accessed | tf_op | source)
XLA Modules:
  0.0 253.8 jit_solution(5773878891755166815)
XLA Ops:
  6.5 0.7 exp.13
  7.3 0.8 fusion.57
  8.1 1.1 fusion.42
  9.2 1.1 fusion.46
  10.3 0.9 subtract_add_fusion.6
  11.2 1.0 add_add_fusion.5
  14.8 0.8 reshape.198
  15.6 13.7 %all-to-all-start = ((f32[32,1,1024]{2,1,0:T(1,128)}), f32[32,1,1024]{2,1,0:T(1,128)S(1)}, u32[]{:S(2)}, u32[]{:S(2)}) async-start(f32[32,1,1024]{2,1,0:T(1,128)} %reshape.198), calls=%async_computation | async-start | bytes 262144 | tf_op jit(solution)/shard_map/all_to_all | solution.py:12
  29.5 9.2 %all-to-all-done = f32[32,1,1024]{2,1,0:T(1,128)S(1)} async-done(((f32[32,1,1024]{2,1,0:T(1,128)}), f32[32,1,1024]{2,1,0:T(1,128)S(1)}, u32[]{:S(2)}, u32[]{:S(2)}) %all-to-all-start) | async-done | bytes 131104 | tf_op jit(solution)/shard_map/all_to_all | solution.py:12
  38.7 0.5 broadcast.191
  39.2 0.9 reduce.12
  41.3 0.5 convolution_convert_fusion.1
  41.8 1.1 copy.117
  42.9 9.3 %all-to-all-start.1 = ((bf16[16,128,256]{2,1,0:T(8,128)(2,1)}), bf16[16,128,256]{2,1,0:T(8,128)(2,1)S(1)}, u32[]{:S(2)}, u32[]{:S(2)}) async-start(bf16[16,128,256]{2,1,0:T(8,128)(2,1)} %bitcast.68), calls=%async_computation.1 | async-start | bytes 2097152 | tf_op jit(solution)/shard_map/all_to_all | solution.py:61
  52.6 0.6 reduce-window.6
  53.9 26.3 %all-to-all-done.1 = bf16[16,128,256]{2,1,0:T(8,128)(2,1)S(1)} async-done(((bf16[16,128,256]{2,1,0:T(8,128)(2,1)}), bf16[16,128,256]{2,1,0:T(8,128)(2,1)S(1)}, u32[]{:S(2)}, u32[]{:S(2)}) %all-to-all-start.1) | async-done | bytes 1048608 | tf_op jit(solution)/shard_map/all_to_all | solution.py:61
  80.3 0.9 add_convert_fusion
  81.3 0.6 broadcast_in_dim.86
  81.9 3.4 %all-to-all-start.2 = ((f32[16,1,128]{2,1,0:T(1,128)}), f32[16,1,128]{2,1,0:T(1,128)S(1)}, u32[]{:S(2)}, u32[]{:S(2)}) async-start(f32[16,1,128]{2,1,0:T(1,128)} %broadcast_in_dim.86), calls=%async_computation.2 | async-start | bytes 16384 | tf_op jit(solution)/shard_map/all_to_all | solution.py:12
  85.4 0.8 dynamic_slice.7
  86.3 6.1 %all-to-all-done.2 = f32[16,1,128]{2,1,0:T(1,128)S(1)} async-done(((f32[16,1,128]{2,1,0:T(1,128)}), f32[16,1,128]{2,1,0:T(1,128)S(1)}, u32[]{:S(2)}, u32[]{:S(2)}) %all-to-all-start.2) | async-done | bytes 8224 | tf_op jit(solution)/shard_map/all_to_all | solution.py:12
  92.4 2.0 gather_fusion
  94.5 15.2 %all_to_all.26 = bf16[32,16,256]{2,1,0:T(8,128)(2,1)} all-to-all(bf16[32,16,256]{2,1,0:T(8,128)(2,1)S(1)} %broadcast_select_fusion), channel_id=1, replica_groups=mesh['sp'=32,'tp'=16] {'sp'}, dimensions={0} | all-to-all | bytes 524288 | tf_op jit(solution)/shard_map/all_to_all | solution.py:204
  109.8 44.8 %all-gather.2.cloned.1.call-done = bf16[32,16,4096]{2,1,0:T(8,128)(2,1)} async-done(((bf16[32,16,256]{2,1,0:T(8,128)(2,1)}), bf16[32,16,4096]{2,1,0:T(8,128)(2,1)}) %all-gather.2.cloned.1.call-update) | async-done | bytes 4194320 | tf_op jit(solution)/shard_map/all_gather | solution.py:205
  154.6 3.6 %fusion.5 = f32[32,16,128]{2,1,0:T(8,128)S(1)} fusion(bf16[32,16,4096]{2,1,0:T(8,128)(2,1)} %all-gather.2.cloned.1.call-done, bf16[1,4096,128]{2,1,0:T(8,128)(2,1)S(1)} %copy-done.2), kind=kOutput, calls=%fused_computation.12 | convolution fusion | flops 536870912 | bytes 5505024 | tf_op jit(solution)/shard_map/snd,df->snf/dot_general | solution.py:206
  158.2 2.5 fusion
  160.7 3.2 %convolution_convert_fusion = bf16[512,4096]{1,0:T(8,128)(2,1)} fusion(bf16[512,128]{1,0:T(8,128)(2,1)S(1)} %bitcast.140, bf16[1,128,4096]{2,1,0:T(8,128)(2,1)S(1)} %copy-done), kind=kOutput, calls=%fused_computation.2 | convolution fusion | flops 538968064 | bytes 5373952 | tf_op jit(solution)/shard_map/dot_general | solution.py:210
  164.2 61.1 %reduce-scatter.2.cloned.1.call-done = bf16[512,256]{1,0:T(8,128)(2,1)} async-done(((bf16[512,4096]{1,0:T(8,128)(2,1)}), bf16[512,256]{1,0:T(8,128)(2,1)}) %reduce-scatter.2.cloned.1.call-update) | async-done | bytes 262160 | tf_op jit(solution)/shard_map/reduce_scatter | solution.py:211
  225.3 8.9 %all-to-all-start.4 = ((bf16[32,16,256]{2,1,0:T(8,128)(2,1)}), bf16[32,16,256]{2,1,0:T(8,128)(2,1)S(1)}, u32[]{:S(2)}, u32[]{:S(2)}) async-start(bf16[32,16,256]{2,1,0:T(8,128)(2,1)} %bitcast.141), calls=%async_computation.5 | async-start | bytes 524288 | tf_op jit(solution)/shard_map/all_to_all | solution.py:215
  234.4 10.3 %all-to-all-done.4 = bf16[32,16,256]{2,1,0:T(8,128)(2,1)S(1)} async-done(((bf16[32,16,256]{2,1,0:T(8,128)(2,1)}), bf16[32,16,256]{2,1,0:T(8,128)(2,1)S(1)}, u32[]{:S(2)}, u32[]{:S(2)}) %all-to-all-start.4) | async-done | bytes 262176 | tf_op jit(solution)/shard_map/all_to_all | solution.py:215
  244.7 1.2 gather_fusion.1
  246.3 0.6 fusion.11
  (81 shorter events, 6.3 us)
Async XLA Ops:
  6.5 154.2 %copy-start = (bf16[1,128,4096]{2,1,0:T(8,128)(2,1)S(1)}, bf16[1,128,4096]{2,1,0:T(8,128)(2,1)}, u32[]{:S(2)}) copy-start(bf16[1,128,4096]{2,1,0:T(8,128)(2,1)} %param.35) | copy-start | bytes 3145732
  13.0 16.3 %copy-start.9 = (f32[64]{0:T(128)S(1)}, f32[64]{0:T(128)}, u32[]{:S(2)}) copy-start(f32[64]{0:T(128)} %param.26) | copy-start | bytes 772
  13.4 27.2 %copy-start.5 = (f32[4,16,64]{2,1,0:T(8,128)S(1)}, f32[4,16,64]{2,1,0:T(8,128)}, u32[]{:S(2)}) copy-start(f32[4,16,64]{2,1,0:T(8,128)} %param.24) | copy-start | bytes 49156
  13.4 27.5 %copy-start.4 = (bf16[64,128]{1,0:T(8,128)(2,1)S(1)}, bf16[64,128]{1,0:T(8,128)(2,1)}, u32[]{:S(2)}) copy-start(bf16[64,128]{1,0:T(8,128)(2,1)} %param.18) | copy-start | bytes 49156
  13.4 27.5 %copy-start.6 = (f32[4,16,64]{2,1,0:T(8,128)S(1)}, f32[4,16,64]{2,1,0:T(8,128)}, u32[]{:S(2)}) copy-start(f32[4,16,64]{2,1,0:T(8,128)} %param.25) | copy-start | bytes 49156
  13.7 27.6 %copy-start.3 = (bf16[64,4096]{1,0:T(8,128)(2,1)S(1)}, bf16[64,4096]{1,0:T(8,128)(2,1)}, u32[]{:S(2)}) copy-start(bf16[64,4096]{1,0:T(8,128)(2,1)} %param.28) | copy-start | bytes 1572868
  15.6 23.1 %all-to-all-start = ((f32[32,1,1024]{2,1,0:T(1,128)}), f32[32,1,1024]{2,1,0:T(1,128)S(1)}, u32[]{:S(2)}, u32[]{:S(2)}) async-start(f32[32,1,1024]{2,1,0:T(1,128)} %reshape.198), calls=%async_computation | async-start | bytes 262144 | tf_op jit(solution)/shard_map/all_to_all | solution.py:12
  40.2 12.0 %copy-start.7 = (s32[128,2]{0,1:T(2,128)S(1)}, s32[128,2]{0,1:T(2,128)}, u32[]{:S(2)}) copy-start(s32[128,2]{0,1:T(2,128)} %param.31) | copy-start | bytes 3076
  42.9 111.7 %copy-start.2 = (bf16[1,4096,128]{2,1,0:T(8,128)(2,1)S(1)}, bf16[1,4096,128]{2,1,0:T(8,128)(2,1)}, u32[]{:S(2)}) copy-start(bf16[1,4096,128]{2,1,0:T(8,128)(2,1)} %param.33) | copy-start | bytes 3145732
  42.9 37.3 %all-to-all-start.1 = ((bf16[16,128,256]{2,1,0:T(8,128)(2,1)}), bf16[16,128,256]{2,1,0:T(8,128)(2,1)S(1)}, u32[]{:S(2)}, u32[]{:S(2)}) async-start(bf16[16,128,256]{2,1,0:T(8,128)(2,1)} %bitcast.68), calls=%async_computation.1 | async-start | bytes 2097152 | tf_op jit(solution)/shard_map/all_to_all | solution.py:61
  81.9 10.4 %all-to-all-start.2 = ((f32[16,1,128]{2,1,0:T(1,128)}), f32[16,1,128]{2,1,0:T(1,128)S(1)}, u32[]{:S(2)}, u32[]{:S(2)}) async-start(f32[16,1,128]{2,1,0:T(1,128)} %broadcast_in_dim.86), calls=%async_computation.2 | async-start | bytes 16384 | tf_op jit(solution)/shard_map/all_to_all | solution.py:12
  85.3 69.3 %all-gather.2.cloned.1.call-start = ((), (), s32[]{:S(2)}) async-start(), calls=%async_computation.6 | async-start | bytes 4456448 | tf_op jit(solution)/shard_map/all_gather | solution.py:205
  109.8 115.5 %reduce-scatter.2.cloned.1.call-start = ((), (), s32[]{:S(2)}) async-start(), calls=%async_computation.7 | async-start | bytes 4456448 | tf_op jit(solution)/shard_map/reduce_scatter | solution.py:211
  154.6 3.6 %copy-start.1 = (bf16[32,16,4096]{2,1,0:T(8,128)(2,1)S(1)}, bf16[32,16,4096]{2,1,0:T(8,128)(2,1)}, u32[]{:S(2)}) copy-start(bf16[32,16,4096]{2,1,0:T(8,128)(2,1)} %all-gather.2.cloned.1.call-done) | copy-start | bytes 12582916
  160.7 3.5 %copy-start.8 = (f32[128,2]{0,1:T(2,128)S(1)}, f32[128,2]{0,1:T(2,128)}, u32[]{:S(2)}) copy-start(f32[128,2]{0,1:T(2,128)} %param.32) | copy-start | bytes 3076
  225.3 19.4 %all-to-all-start.4 = ((bf16[32,16,256]{2,1,0:T(8,128)(2,1)}), bf16[32,16,256]{2,1,0:T(8,128)(2,1)S(1)}, u32[]{:S(2)}, u32[]{:S(2)}) async-start(bf16[32,16,256]{2,1,0:T(8,128)(2,1)} %bitcast.141), calls=%async_computation.5 | async-start | bytes 524288 | tf_op jit(solution)/shard_map/all_to_all | solution.py:215
Sparse Core Ops, SparseCore 0:
  109.9 44.6 all-gather.1
  164.0 61.1 reduce-scatter.1
where the time goes:
time: 257 us; the launch traced here: 254 us
  waiting for transfers between devices  158 us (61%)
  starting transfers between devices  35.4 us (14%)
  blocking collectives  15.2 us (6%)
  between operations  13.9 us (5%)
  matrix products  12.5 us (5%)
  local copies, waits for them, and re-layouts  9.55 us (4%)
  other arithmetic  9.4 us (4%)
    reduce_scatter x1, waiting for transfers between devices, per_device(): lax.psum_scatter(down_part.astype(f32).astype(jnp.bfloat16), 'tp', scatte...  61.1 us
    all_gather x1, waiting for transfers between devices, per_device(): piece = lax.all_gather(arrived, 'tp', axis=2, tiled=True)  44.8 us
    all_to_all x1, waiting for transfers between devices, sent_and_summed(): lax.all_to_all(in_blocks(array, dim, length), axis, 0, 0, tiled=True)  26.3 us
    all_to_all x2, starting transfers between devices, copy_for_each(): return lax.all_to_all(copies, axis, split_axis=0, concat_axis=0, tiled=True)  17.1 us
    all_to_all x2, waiting for transfers between devices, copy_for_each(): return lax.all_to_all(copies, axis, split_axis=0, concat_axis=0, tiled=True)  15.3 us
    all_to_all x1, blocking collectives, per_device(): lax.all_to_all(dispatch, 'sp', split_axis=0, concat_axis=0, tiled=True)  15.2 us
    all_to_all x1, waiting for transfers between devices, per_device(): lax.all_to_all(expert_out, 'sp', split_axis=0, concat_axis=0, tiled=True)  10.3 us
    all_to_all x1, starting transfers between devices, sent_and_summed(): lax.all_to_all(in_blocks(array, dim, length), axis, 0, 0, tiled=True)  9.3 us
  transfers between devices with their start and end apart: 6, of which 6 were waited for; matrix products, arithmetic and copies ran while one was open for 1% of the time, Pallas kernels for 0%

commit v1 on v0

v1 whole, which is shorter than its diff:
```python
import functools

import jax
import jax.numpy as jnp
from jax import lax
from jax.experimental import pallas as pl
from jax.experimental.pallas import tpu as pltpu
from jax.sharding import PartitionSpec as P

EPS = 1e-06
HIGH = lax.Precision.HIGHEST
MESH = pl.DeviceIdType.MESH
F32 = jnp.float32
BF16 = jnp.bfloat16
CORES = 2
CHUNKS = 4
SKEW = 1


def iota(shape, dim):
    return lax.broadcasted_iota(jnp.int32, shape, dim)


def to_col(row):
    n = row.shape[1]
    eye = iota((n, n), 0) == iota((n, n), 1)
    return jnp.sum(jnp.where(eye, row, 0.0), axis=1, keepdims=True)


def to_row(col):
    n = col.shape[0]
    eye = iota((n, n), 0) == iota((n, n), 1)
    return jnp.sum(jnp.where(eye, col, 0.0), axis=0, keepdims=True)


def small_expm1(x):
    total = jnp.ones_like(x)
    for k in range(11, 1, -1):
        total = 1.0 + total * x * (1.0 / k)
    return jnp.where(x > -0.7, x * total, jnp.exp(x) - 1.0)


def times(ar, ai, br, bi):
    return ar * br - ai * bi, ar * bi + ai * br


def mixer_kernel(
    dims,
    u_ref, damp_ref, ang_ref, ie_ref, ein_ref, eq_ref, cin_ref, cq_ref, byp_ref, off_ref,
    sel_ref, score_ref, wexit_hbm, skip_hbm, gain_hbm, gate_hbm, up_hbm, down_hbm,
    out_ref,
    msg, heads, wx, mx, dw, gu, skip, gain, ss, inv, rinv, disp, whi, wlo,
    xs, g_buf, h_buf, acc, oacc, outb, ret, stream_s, loc_r, cum_r, cum_i,
    l_sem, s_pre, r_pre, s_wx, r_wx, s_mx, r_mx, s_dw, r_dw, s_ss, r_ss,
    s_inv, r_inv, s_dis, r_dis, s_ret, r_ret, s_g, r_g, s_h, r_h,
):
    n_sp, n_tp, groups, states, lanes, tok, width, cap = dims
    n_y = n_tp // CORES
    d_local = width // n_tp
    f_local = gate_hbm.shape[2]
    slots = n_sp * cap
    rows_q = slots // CHUNKS
    sp_q = n_sp // CHUNKS
    me, mt = lax.axis_index("sp"), lax.axis_index("tp")
    y, core = mt // CORES, mt % CORES
    twin = y * CORES + (1 - core)

    def each(count, mine, fn):
        def step(j, carry):
            fn(lax.rem(mine + j, count))
            return carry
        lax.fori_loop(1, count, step, 0)

    def span(lo, hi, fn):
        def step(j, carry):
            fn(j)
            return carry
        lax.fori_loop(lo, hi, step, 0)

    def remote(src, dst, send, recv, sp, tp):
        return pltpu.make_async_remote_copy(
            src_ref=src, dst_ref=dst, send_sem=send, recv_sem=recv,
            device_id=(sp, tp), device_id_type=MESH)

    heads[...] = jnp.zeros_like(heads)
    barrier = pltpu.get_barrier_semaphore()
    each(n_sp, me, lambda k: pl.semaphore_signal(
        barrier, inc=1, device_id=(k, mt), device_id_type=MESH))
    each(n_tp, mt, lambda k: pl.semaphore_signal(
        barrier, inc=1, device_id=(me, k), device_id_type=MESH))

    own_cols = pl.ds(pl.multiple_of(mt * d_local, d_local), d_local)
    chan = groups * lanes
    local = [
        pltpu.make_async_copy(skip_hbm.at[:, own_cols], skip, l_sem.at[0]),
        pltpu.make_async_copy(gain_hbm.at[:, own_cols], gain, l_sem.at[1]),
        pltpu.make_async_copy(wexit_hbm.at[:, own_cols], wx.at[mt], l_sem.at[2]),
        pltpu.make_async_copy(gate_hbm.at[0], gu.at[:, pl.ds(0, f_local)], l_sem.at[3]),
        pltpu.make_async_copy(up_hbm.at[0], gu.at[:, pl.ds(f_local, f_local)], l_sem.at[4]),
        pltpu.make_async_copy(down_hbm.at[0, :, own_cols], dw.at[mt], l_sem.at[5]),
    ]
    for copy in local:
        copy.start()

    step_size = jnp.exp(to_col(ie_ref[...]))
    damp, ang = damp_ref[...], ang_ref[...]
    rate, angle = damp * step_size, ang * step_size
    cos, sin = jnp.cos(angle), jnp.sin(angle)
    half = jnp.sin(0.5 * angle)
    num_re = small_expm1(rate) * cos - 2.0 * half * half
    num_im = jnp.exp(rate) * sin
    denom = damp * damp + ang * ang
    fac_re = (num_re * damp + num_im * ang) / denom
    fac_im = (num_im * damp - num_re * ang) / denom
    total = off_ref[...]
    lane_g = iota(total.shape, 1)
    shift = 1
    while shift < tok:
        total = total + jnp.where(lane_g >= shift, pltpu.roll(total, shift, 1), 0.0)
        shift *= 2
    lane = iota((states, tok), 1)
    bypass = byp_ref[...]
    for g in range(groups):
        row = slice(g, g + 1)
        u = u_ref[g * lanes:(g + 1) * lanes, :].astype(F32)
        e_re = jnp.dot(ein_ref[g], u, precision=HIGH, preferred_element_type=F32)
        e_im = jnp.dot(eq_ref[g], u, precision=HIGH, preferred_element_type=F32)
        f_re, f_im = to_col(fac_re[row]), to_col(fac_im[row])
        s_re, s_im = times(f_re, f_im, e_re, e_im)
        rate_c = to_col(rate[row])
        w_re, w_im = to_col(cos[row]), to_col(sin[row])
        sums = total[row]
        p_re, p_im = jnp.ones((states, tok), F32), jnp.zeros((states, tok), F32)
        shift = 1
        while shift <= tok:
            taken = (jnp.bitwise_and(lane + 1, shift)) != 0
            q_re, q_im = times(p_re, p_im, w_re, w_im)
            p_re, p_im = jnp.where(taken, q_re, p_re), jnp.where(taken, q_im, p_im)
            if shift < tok:
                gap = sums - pltpu.roll(sums, shift, 1)
                size = jnp.exp(rate_c * float(shift) + jnp.minimum(gap, 0.0))
                size = jnp.where(lane >= shift, size, 0.0)
                t_re, t_im = times(
                    w_re, w_im, pltpu.roll(s_re, shift, 1), pltpu.roll(s_im, shift, 1))
                s_re, s_im = s_re + size * t_re, s_im + size * t_im
                w_re, w_im = times(w_re, w_im, w_re, w_im)
            shift *= 2
        size = jnp.exp(rate_c * (lane + 1).astype(F32) + sums)
        cum_r[g], cum_i[g] = size * p_re, size * p_im
        last = lane == tok - 1
        h_re = to_row(jnp.sum(jnp.where(last, s_re, 0.0), axis=1, keepdims=True))
        h_im = to_row(jnp.sum(jnp.where(last, s_im, 0.0), axis=1, keepdims=True))
        end = jnp.sum(jnp.where(lane_g[row] == tok - 1, sums, 0.0), axis=1, keepdims=True)
        msg[g:g + 1, 0:states] = h_re
        msg[g:g + 1, states:2 * states] = jnp.broadcast_to(end, (1, states))
        msg[groups + g:groups + g + 1, 0:states] = h_im
        msg[groups + g:groups + g + 1, states:2 * states] = jnp.zeros((1, states), F32)
        loc_r[g] = (
            jnp.dot(cin_ref[g], s_re, precision=HIGH, preferred_element_type=F32)
            - jnp.dot(cq_ref[g], s_im, precision=HIGH, preferred_element_type=F32)
            + to_col(bypass[:, g * lanes:(g + 1) * lanes]) * u)

    pl.semaphore_wait(barrier, n_sp - 1 + n_tp - 1)

    def send_head(k):
        return remote(msg, heads.at[me], s_pre.at[k], r_pre.at[me], k, mt)

    def head_from(k):
        return remote(msg, heads.at[k], s_pre.at[k], r_pre.at[k], me, mt)

    span(me + 1, n_sp, lambda k: send_head(k).start())

    def columns_of(k):
        return pl.ds(pl.multiple_of(k * d_local, d_local), d_local)

    def send_wx(k):
        return remote(
            wexit_hbm.at[:, columns_of(k)], wx.at[mt], s_wx.at[k], r_wx.at[mt], me, k)

    def send_dw(k):
        return remote(
            down_hbm.at[0, :, columns_of(k)], dw.at[mt], s_dw.at[k], r_dw.at[mt], me, k)

    each(n_tp, mt, lambda k: send_wx(k).start())

    sel, score = sel_ref[...], score_ref[...]
    expert = iota((tok, n_sp), 1)
    hit0 = (sel[:, 0:1] == expert).astype(F32)
    hit1 = (sel[:, 1:2] == expert).astype(F32)
    hits = (hit0 + hit1).astype(BF16)
    below = (iota((tok, tok), 1) < iota((tok, tok), 0)).astype(F32).astype(BF16)
    rank = jnp.dot(below, hits, preferred_element_type=F32).astype(BF16)
    slot_e, slot_j = iota((n_sp, slots), 0), iota((n_sp, slots), 1)
    spread = ((slot_j >= slot_e * cap) & (slot_j < (slot_e + 1) * cap)).astype(F32).astype(BF16)
    hits_x = jnp.dot(hits, spread, preferred_element_type=F32)
    hit0_x = jnp.dot(hit0.astype(BF16), spread, preferred_element_type=F32)
    rank_x = jnp.dot(rank, spread, preferred_element_type=F32)
    place = jnp.bitwise_and(iota((tok, slots), 1), cap - 1).astype(F32)
    picked = (hits_x > 0.5) & (rank_x == place)
    disp[...] = picked.astype(F32).astype(BF16)
    both = score[:, 0:1] + score[:, 1:2]
    share = jnp.where(hit0_x > 0.5, score[:, 0:1] / both, score[:, 1:2] / both)
    share = jnp.where(picked, share, 0.0)
    high = share.astype(BF16)
    whi[...] = high
    wlo[...] = (share - high.astype(F32)).astype(BF16)

    span(0, me, lambda k: head_from(k).wait_recv())
    w_re, w_im = cos, sin
    shift = 1
    while shift < tok:
        w_re, w_im = times(w_re, w_im, w_re, w_im)
        shift *= 2
    in_re, in_im = jnp.zeros_like(rate), jnp.zeros_like(rate)
    for k in range(n_sp - 1):
        head = heads[k]
        size = jnp.exp(rate * float(tok) + head[0:groups, states:2 * states])
        n_re, n_im = times(size * w_re, size * w_im, in_re, in_im)
        n_re = n_re + head[0:groups, 0:states]
        n_im = n_im + head[groups:2 * groups, 0:states]
        in_re = jnp.where(k < me, n_re, in_re)
        in_im = jnp.where(k < me, n_im, in_im)
    for g in range(groups):
        row = slice(g, g + 1)
        c_re, c_im = times(cin_ref[g], cq_ref[g], in_re[row], in_im[row])
        value = (
            loc_r[g]
            + jnp.dot(c_re, cum_r[g], precision=HIGH, preferred_element_type=F32)
            - jnp.dot(c_im, cum_i[g], precision=HIGH, preferred_element_type=F32))
        mx[mt, g * lanes:(g + 1) * lanes, :] = jax.nn.gelu(value).astype(BF16)

    def send_mx(k):
        return remote(mx.at[mt], mx.at[mt], s_mx.at[k], r_mx.at[mt], me, k)

    each(n_tp, mt, lambda k: send_mx(k).start())
    each(n_tp, mt, lambda k: send_dw(k).start())

    def wait_tp(buf, sems):
        each(n_tp, mt, lambda k: remote(
            buf.at[k], buf.at[k], sems.at[k], sems.at[k], me, k).wait_recv())

    local[0].wait()
    local[1].wait()
    local[2].wait()
    wait_tp(wx, r_wx)
    wait_tp(mx, r_mx)
    projected = lax.dot_general(
        mx[...].reshape(n_tp * chan, tok), wx[...].reshape(n_tp * chan, d_local),
        (((0,), (0,)), ((), ())), preferred_element_type=F32).astype(BF16)
    stream = (skip[...].astype(F32) + projected.astype(F32)).astype(BF16)
    stream_f = stream.astype(F32)
    stream_s[...] = stream_f
    squares = to_row(jnp.sum(stream_f * stream_f, axis=1, keepdims=True))
    ss[mt] = jnp.broadcast_to(squares, (8, tok))

    scaled = (stream_f * gain[...]).astype(BF16)
    sent = lax.dot_general(
        disp[...], scaled, (((0,), (0,)), ((), ())),
        preferred_element_type=F32).astype(BF16).reshape(n_sp, cap, d_local)
    xs[...] = sent

    def rows_of(k):
        return pl.ds(pl.multiple_of(k * cap, cap), cap)

    def send_rows(k):
        return remote(
            xs.at[k], g_buf.at[mt, rows_of(me), :], s_dis.at[k], r_dis.at[me], k, mt)

    each(n_sp, me, lambda k: send_rows(k).start())
    own_rows = pltpu.make_async_copy(xs.at[me], g_buf.at[mt, rows_of(me), :], l_sem.at[6])
    own_rows.start()

    def send_ss(k):
        return remote(ss.at[mt], ss.at[mt], s_ss.at[k], r_ss.at[mt], me, k)

    each(n_tp, mt, lambda k: send_ss(k).start())
    wait_tp(ss, r_ss)
    norm = lax.rsqrt(jnp.sum(ss[...], axis=0)[0:1, :] * (1.0 / width) + EPS)
    norm_x = jnp.sum(disp[...].astype(F32) * to_col(norm), axis=0, keepdims=True)
    for k in range(slots // 128):
        inv[k] = jnp.broadcast_to(norm_x[:, k * 128:(k + 1) * 128], (8, 128))

    def tile_of(k):
        return (k * cap) // 128

    def send_inv(k):
        return remote(
            inv.at[tile_of(k)], rinv.at[me], s_inv.at[k], r_inv.at[me], k, mt)

    each(n_sp, me, lambda k: send_inv(k).start())
    rinv[me] = inv[tile_of(me)]

    def inv_of(q):
        part = rinv[q * sp_q:(q + 1) * sp_q]
        full = jnp.concatenate([part] * (cap // 8), axis=1).reshape(rows_q, 128)
        want = (me * cap) % 128 + jnp.bitwise_and(iota((rows_q, 128), 0), cap - 1)
        return jnp.sum(jnp.where(iota((rows_q, 128), 1) == want, full, 0.0), axis=1, keepdims=True)

    def hops(q):
        far, near = n_y // 2, n_y - 1 - n_y // 2
        return (far, near) if q % 2 == 0 else (near, far)

    deepest = n_y // 2

    def chip(k):
        return lax.rem(y + k + n_y, n_y)

    started = []

    def ring_hop(buf, send, recv, q, h):
        rows = pl.ds(q * rows_q, rows_q)

        def push(owner, tp, slot):
            copy = remote(
                buf.at[owner, rows, :], buf.at[owner, rows, :],
                send.at[slot, q], recv.at[owner, q], me, tp)
            copy.start()
            started.append(copy)

        def arrived(owner):
            remote(
                buf.at[owner, rows, :], buf.at[owner, rows, :],
                send.at[0, q], recv.at[owner, q], me, mt).wait_recv()

        right, left = hops(q)
        right_tp, left_tp = chip(1) * CORES + core, chip(-1) * CORES + core
        if h == 0:
            push(mt, right_tp, 0)
            push(mt, left_tp, 1)
            push(mt, twin, 2)
            return
        if h <= right:
            owner = chip(-h) * CORES + core
            arrived(owner)
            if h < right:
                push(owner, right_tp, 3 * h)
            push(owner, twin, 3 * h + 2)
        if h <= left:
            owner = chip(h) * CORES + core
            arrived(owner)
            if h < left:
                push(owner, left_tp, 3 * h + 1)
            push(owner, twin, 3 * (deepest + 1) + h)

    def pairs(buf, send, recv, q, h, weights, target, deep):
        rows = pl.ds(q * rows_q, rows_q)
        right, left = hops(q)
        owners = [0] if h == 0 else [-h] * (h <= right) + [h] * (h <= left)
        for k in owners:
            there = chip(k)
            other = there * CORES + (1 - core)
            remote(
                buf.at[other, rows, :], buf.at[other, rows, :],
                send.at[0, q], recv.at[other, q], me, mt).wait_recv()
            both = jnp.concatenate(
                [buf[there * CORES, rows, :], buf[there * CORES + 1, rows, :]], axis=1)
            part = jnp.dot(both, weights(there), preferred_element_type=F32)
            if h == 0:
                target[rows, :] = part
            else:
                target[rows, :] += part

    def gate_up(there):
        depth = CORES * d_local
        return gu[pl.ds(pl.multiple_of(there * depth, depth), depth), :]

    def down(there):
        return jnp.concatenate([dw[there * CORES], dw[there * CORES + 1]], axis=0)

    def send_back(k):
        return remote(
            outb.at[rows_of(k), :], ret.at[rows_of(me), :], s_ret.at[k], r_ret.at[me], k, mt)

    own_back = pltpu.make_async_copy(
        outb.at[rows_of(me), :], ret.at[rows_of(me), :], l_sem.at[7])

    def stage(q, st):
        rows = slice(q * rows_q, (q + 1) * rows_q)
        first = deepest + 1
        if st == 0:
            def got(k):
                @pl.when(k != me)
                def _():
                    remote(
                        xs.at[0], g_buf.at[mt, rows_of(k), :], s_dis.at[k], r_dis.at[k],
                        me, mt).wait_recv()

                @pl.when(k == me)
                def _():
                    own_rows.wait()
            span(q * sp_q, (q + 1) * sp_q, got)
            ring_hop(g_buf, s_g, r_g, q, 0)
        elif st <= deepest:
            ring_hop(g_buf, s_g, r_g, q, st)
            pairs(g_buf, s_g, r_g, q, st - 1, gate_up, acc, None)
        elif st == first:
            pairs(g_buf, s_g, r_g, q, deepest, gate_up, acc, None)
            factor = inv_of(q)
            gate = acc[rows, 0:f_local] * factor
            wide = acc[rows, f_local:2 * f_local] * factor
            h_buf[mt, rows, :] = (jax.nn.silu(gate) * wide).astype(BF16)
            ring_hop(h_buf, s_h, r_h, q, 0)
        elif st <= first + deepest:
            ring_hop(h_buf, s_h, r_h, q, st - first)
            pairs(h_buf, s_h, r_h, q, st - first - 1, down, oacc, None)
        else:
            pairs(h_buf, s_h, r_h, q, deepest, down, oacc, None)
            outb[rows, :] = oacc[rows, :].astype(BF16)

            def back(k):
                @pl.when(k != me)
                def _():
                    send_back(k).start()

                @pl.when(k == me)
                def _():
                    own_back.start()
            span(q * sp_q, (q + 1) * sp_q, back)

    last_stage = 2 * deepest + 2
    order = sorted((st + SKEW * q, q, st) for q in range(CHUNKS) for st in range(last_stage + 1))
    ready = {0: False, 1: False}
    for _, q, st in order:
        if st == 1 and not ready[0]:
            local[3].wait()
            local[4].wait()
            ready[0] = True
        if st == deepest + 1 and not ready[1]:
            each(n_sp, me, lambda k: remote(
                inv.at[0], rinv.at[k], s_inv.at[k], r_inv.at[k], me, mt).wait_recv())
            local[5].wait()
            wait_tp(dw, r_dw)
            ready[1] = True
        stage(q, st)

    own_back.wait()
    each(n_sp, me, lambda k: remote(
        outb.at[rows_of(k), :], ret.at[rows_of(k), :], s_ret.at[k], r_ret.at[k],
        me, mt).wait_recv())
    back = ret[...]
    out_ref[...] = (
        stream_s[...]
        + jnp.dot(whi[...], back, preferred_element_type=F32)
        + jnp.dot(wlo[...], back, preferred_element_type=F32)).astype(BF16)

    span(me + 1, n_sp, lambda k: send_head(k).wait_send())
    for fn in (send_wx, send_mx, send_dw, send_ss):
        each(n_tp, mt, lambda k: fn(k).wait_send())
    for fn in (send_rows, send_inv, send_back):
        each(n_sp, me, lambda k: fn(k).wait_send())
    for copy in started:
        copy.wait_send()


def per_device(
    lane_source_signal, spectral_damping_part, spectral_angular_part, interval_exponent,
    entry_matrix_inphase, entry_matrix_quadrature, emission_inphase, emission_quadrature,
    lane_bypass_factor, spike_shrink_offset, lane_exit_matrix, skipline_stream,
    specialist_scaling_vector, selected_specialists, dispatcher_scores,
    specialist_valve_matrix, specialist_widen_matrix, specialist_shrink_matrix,
):
    n_sp, n_tp = lax.axis_size("sp"), lax.axis_size("tp")
    groups, states, lanes = entry_matrix_inphase.shape
    chan, tok = lane_source_signal.shape
    width = specialist_scaling_vector.shape[0]
    d_local = width // n_tp
    f_local = specialist_valve_matrix.shape[2]
    cap = 2 * tok * selected_specialists.shape[1] // n_sp
    slots = n_sp * cap
    deepest = n_tp // CORES // 2
    dims = (n_sp, n_tp, groups, states, lanes, tok, width, cap)
    vmem = pl.BlockSpec(memory_space=pltpu.VMEM)
    hbm = pl.BlockSpec(memory_space=pl.ANY)
    dma = pltpu.SemaphoreType.DMA
    scratch = [
        pltpu.VMEM((8, 128), F32),
        pltpu.VMEM((n_sp, 8, 128), F32),
        pltpu.VMEM((n_tp, chan, d_local), BF16),
        pltpu.VMEM((n_tp, chan, tok), BF16),
        pltpu.VMEM((n_tp, f_local, d_local), BF16),
        pltpu.VMEM((width, 2 * f_local), BF16),
        pltpu.VMEM((tok, d_local), BF16),
        pltpu.VMEM((1, d_local), F32),
        pltpu.VMEM((n_tp, 8, tok), F32),
        pltpu.VMEM((slots // 128, 8, 128), F32),
        pltpu.VMEM((n_sp, 8, 128), F32),
        pltpu.VMEM((tok, slots), BF16),
        pltpu.VMEM((tok, slots), BF16),
        pltpu.VMEM((tok, slots), BF16),
        pltpu.VMEM((n_sp, cap, d_local), BF16),
        pltpu.VMEM((n_tp, slots, d_local), BF16),
        pltpu.VMEM((n_tp, slots, f_local), BF16),
        pltpu.VMEM((slots, 2 * f_local), F32),
        pltpu.VMEM((slots, d_local), F32),
        pltpu.VMEM((slots, d_local), BF16),
        pltpu.VMEM((slots, d_local), BF16),
        pltpu.VMEM((tok, d_local), F32),
        pltpu.VMEM((groups, lanes, tok), F32),
        pltpu.VMEM((groups, states, tok), F32),
        pltpu.VMEM((groups, states, tok), F32),
        dma((8,)),
        dma((n_sp,)), dma((n_sp,)),
        dma((n_tp,)), dma((n_tp,)), dma((n_tp,)), dma((n_tp,)),
        dma((n_tp,)), dma((n_tp,)), dma((n_tp,)), dma((n_tp,)),
        dma((n_sp,)), dma((n_sp,)), dma((n_sp,)), dma((n_sp,)), dma((n_sp,)), dma((n_sp,)),
        dma((4 * deepest + 4, CHUNKS)), dma((n_tp, CHUNKS)),
        dma((4 * deepest + 4, CHUNKS)), dma((n_tp, CHUNKS)),
    ]
    return pl.pallas_call(
        functools.partial(mixer_kernel, dims),
        out_shape=jax.ShapeDtypeStruct((tok, d_local), BF16),
        in_specs=[vmem] * 12 + [hbm] * 6,
        out_specs=vmem,
        scratch_shapes=scratch,
        compiler_params=pltpu.CompilerParams(
            collective_id=0, has_side_effects=True, vmem_limit_bytes=60 * 1024 * 1024),
    )(
        lane_source_signal, spectral_damping_part, spectral_angular_part,
        interval_exponent.reshape(1, groups), entry_matrix_inphase, entry_matrix_quadrature,
        emission_inphase, emission_quadrature, lane_bypass_factor.reshape(1, chan),
        spike_shrink_offset, selected_specialists, dispatcher_scores, lane_exit_matrix,
        skipline_stream, specialist_scaling_vector.reshape(1, width),
        specialist_valve_matrix, specialist_widen_matrix, specialist_shrink_matrix,
    )


def solution(mesh):
    placed = (
        P("tp", "sp"), P("tp", None), P("tp", None), P("tp"), P("tp", None, None),
        P("tp", None, None), P("tp", None, None), P("tp", None, None), P("tp"),
        P("tp", "sp"), P("tp", None), P("sp", None), P(), P("sp", None), P("sp", None),
        P("sp", None, "tp"), P("sp", None, "tp"), P("sp", "tp", None),
    )
    return jax.shard_map(
        per_device, mesh=mesh, in_specs=placed, out_specs=P("sp", "tp"), check_vma=False
    )
```

time: 257 us -> 126 us (0.49); the launches traced: 254 us -> 126 us
  waiting for transfers between devices: 158 us -> 0 us
  Pallas kernels: 0 us -> 120 us
  starting transfers between devices: 35.4 us -> 0 us
  blocking collectives: 15.2 us -> 0 us
  between operations: 13.9 us -> 0.02 us
  matrix products: 12.5 us -> 0 us
  other arithmetic: 9.4 us -> 0 us
  local copies, waits for them, and re-layouts: 9.55 us -> 5.15 us
    pallas_call x0 -> x1, Pallas kernels: none -> 120 us  [per_device(): pl.pallas_call(functools.partial(mixer_kernel, dims), out_shape=jax.Shape...]
    reduce_scatter x1 -> x0, waiting for transfers between devices: 61.1 us -> none  [per_device(): lax.psum_scatter(down_part.astype(f32).astype(jnp.bfloat16), 'tp', scatte...]
    all_to_all x4 -> x0, waiting for transfers between devices: 51.9 us -> none  [the longest x1 26.3 us: sent_and_summed(): lax.all_to_all(in_blocks(array, dim, length), axis, 0, 0, tiled=True)]
    all_gather x1 -> x0, waiting for transfers between devices: 44.8 us -> none  [per_device(): piece = lax.all_gather(arrived, 'tp', axis=2, tiled=True)]
    all_to_all x4 -> x0, starting transfers between devices: 35.4 us -> none  [the longest x2 17.1 us: copy_for_each(): return lax.all_to_all(copies, axis, split_axis=0, concat_axis=0, tiled=True)]
    all_to_all x1 -> x0, blocking collectives: 15.2 us -> none  [per_device(): lax.all_to_all(dispatch, 'sp', split_axis=0, concat_axis=0, tiled=True)]
    dot_general x8 -> x0, matrix products: 12.5 us -> none  [the longest x1 3.59 us: per_device(): jnp.einsum('snd,df->snf', piece, gate_w, preferred_element_type=f32)]
    unnamed x23 -> x13, local copies, waits for them, and re-layouts: 1.09 us -> 5.15 us
  transfers between devices with their start and end apart: 6 -> 0, of which waited for: 6 -> 0; matrix products, arithmetic and copies ran while one was open for 1% -> 0% of each run, Pallas kernels for 0% -> 0%
where the time goes in v1:
time: 126 us
  Pallas kernels  120 us (95%)
  local copies, waits for them, and re-layouts  5.15 us (4%)
    pallas_call x1, Pallas kernels, per_device(): pl.pallas_call(functools.partial(mixer_kernel, dims), out_shape=jax.Shape...  120 us
    unnamed x13, local copies, waits for them, and re-layouts  5.15 us

profile of v1, /device:TPU:1, one launch (start us, length us, event | category | flops | bytes accessed | tf_op | source)
XLA Modules:
  0.0 125.6 jit_solution(350372830557794751)
XLA Ops:
  0.0 0.0 copy-start.2
  0.0 0.7 copy-done.2
  0.7 0.0 copy-start.3
  0.7 0.7 copy.21.sel_ref
  1.4 0.0 copy-done.3
  1.4 0.0 copy-start
  1.4 0.7 copy.22.score_ref
  2.2 0.0 copy-done
  2.2 0.0 copy-start.1
  2.2 0.7 copy.19.ein_ref
  2.9 0.0 copy-done.1
  2.9 0.7 copy.20.eq_ref
  3.7 120.4 %shard_map.172 = bf16[128,256]{1,0:T(8,128)(2,1)} custom-call(bf16[64,128]{1,0:T(8,128)(2,1)} %u_ref.1, f32[4,64]{1,0:T(4,128)} %damp_ref.1, f32[4,64]{1,0:T(4,128)} %ang_ref.1, f32[1,4]{1,0:T(1,128)} %bitcast.4, f32[4,64,16]{2,1,0:T(8,128)} %copy.19.ein_ref, f32[4,64,16]{2,1,0:T(8,128)} %copy.20.eq_ref, f32[4,16,64]{2,1,0:T(8,128)} %cin_ref.1, ...), custom_call_target="tpu_custom_call" | custom-call | tf_op jit(solution)/shard_map/pallas_call | solution.py:509
  124.1 1.5 %copy.24 = bf16[128,256]{1,0:T(8,128)(2,1)} copy(bf16[128,256]{1,0:T(8,128)(2,1)} %shard_map.172) | data formatting | bytes 131072
Async XLA Ops:
  0.0 0.7 copy-start.2
  0.7 0.7 copy-start.3
  1.4 0.8 copy-start
  2.2 0.8 copy-start.1

commit v2 on v1

--- a/solution.py
+++ b/solution.py
@@ -14,7 +14,9 @@
 BF16 = jnp.bfloat16
 CORES = 2
 CHUNKS = 4
-SKEW = 1
+SKEW = 0.5
+X_CHIPS = 4
+DW_EARLY = 2
 
 
 def iota(shape, dim):
@@ -38,6 +40,11 @@
     for k in range(11, 1, -1):
         total = 1.0 + total * x * (1.0 / k)
     return jnp.where(x > -0.7, x * total, jnp.exp(x) - 1.0)
+
+
+def dot_first(a, b):
+    return lax.dot_general(
+        a, b, (((0,), (0,)), ((), ())), precision=HIGH, preferred_element_type=F32)
 
 
 def times(ar, ai, br, bi):
@@ -51,7 +58,7 @@
     out_ref,
     msg, heads, wx, mx, dw, gu, skip, gain, ss, inv, rinv, disp, whi, wlo,
     xs, g_buf, h_buf, acc, oacc, outb, ret, stream_s, loc_r, cum_r, cum_i,
-    l_sem, s_pre, r_pre, s_wx, r_wx, s_mx, r_mx, s_dw, r_dw, s_ss, r_ss,
+    l_sem, s_pre, r_pre, s_wx, r_wx, s_wq, r_wq, s_mx, r_mx, s_dw, r_dw, s_ss, r_ss,
     s_inv, r_inv, s_dis, r_dis, s_ret, r_ret, s_g, r_g, s_h, r_h,
 ):
     n_sp, n_tp, groups, states, lanes, tok, width, cap = dims
@@ -64,6 +71,11 @@
     me, mt = lax.axis_index("sp"), lax.axis_index("tp")
     y, core = mt // CORES, mt % CORES
     twin = y * CORES + (1 - core)
+    x_part = me % X_CHIPS
+    away = [k for d in range(1, n_y // 2 + 1) for k in ((d, -d) if 2 * d < n_y else (d,))]
+
+    def chip(k):
+        return lax.rem(y + k + n_y, n_y)
 
     def each(count, mine, fn):
         def step(j, carry):
@@ -81,6 +93,15 @@
         return pltpu.make_async_remote_copy(
             src_ref=src, dst_ref=dst, send_sem=send, recv_sem=recv,
             device_id=(sp, tp), device_id_type=MESH)
+
+    scope = []
+
+    def mark(name):
+        if scope:
+            scope.pop().__exit__(None, None, None)
+        if name:
+            scope.append(jax.named_scope(name))
+            scope[-1].__enter__()
 
     heads[...] = jnp.zeros_like(heads)
     barrier = pltpu.get_barrier_semaphore()
@@ -89,12 +110,16 @@
     each(n_tp, mt, lambda k: pl.semaphore_signal(
         barrier, inc=1, device_id=(me, k), device_id_type=MESH))
 
+    mark("local_copies")
     own_cols = pl.ds(pl.multiple_of(mt * d_local, d_local), d_local)
     chan = groups * lanes
+    part = chan // X_CHIPS
+    quarter = pl.ds(pl.multiple_of(x_part * part, part), part)
     local = [
         pltpu.make_async_copy(skip_hbm.at[:, own_cols], skip, l_sem.at[0]),
         pltpu.make_async_copy(gain_hbm.at[:, own_cols], gain, l_sem.at[1]),
-        pltpu.make_async_copy(wexit_hbm.at[:, own_cols], wx.at[mt], l_sem.at[2]),
+        pltpu.make_async_copy(
+            wexit_hbm.at[quarter, own_cols], wx.at[mt, quarter, :], l_sem.at[2]),
         pltpu.make_async_copy(gate_hbm.at[0], gu.at[:, pl.ds(0, f_local)], l_sem.at[3]),
         pltpu.make_async_copy(up_hbm.at[0], gu.at[:, pl.ds(f_local, f_local)], l_sem.at[4]),
         pltpu.make_async_copy(down_hbm.at[0, :, own_cols], dw.at[mt], l_sem.at[5]),
@@ -102,6 +127,7 @@
     for copy in local:
         copy.start()
 
+    mark("state")
     step_size = jnp.exp(to_col(ie_ref[...]))
     damp, ang = damp_ref[...], ang_ref[...]
     rate, angle = damp * step_size, ang * step_size
@@ -123,8 +149,8 @@
     for g in range(groups):
         row = slice(g, g + 1)
         u = u_ref[g * lanes:(g + 1) * lanes, :].astype(F32)
-        e_re = jnp.dot(ein_ref[g], u, precision=HIGH, preferred_element_type=F32)
-        e_im = jnp.dot(eq_ref[g], u, precision=HIGH, preferred_element_type=F32)
+        e_re = dot_first(ein_ref[g], u)
+        e_im = dot_first(eq_ref[g], u)
         f_re, f_im = to_col(fac_re[row]), to_col(fac_im[row])
         s_re, s_im = times(f_re, f_im, e_re, e_im)
         rate_c = to_col(rate[row])
@@ -160,6 +186,7 @@
             - jnp.dot(cq_ref[g], s_im, precision=HIGH, preferred_element_type=F32)
             + to_col(bypass[:, g * lanes:(g + 1) * lanes]) * u)
 
+    mark("barrier")
     pl.semaphore_wait(barrier, n_sp - 1 + n_tp - 1)
 
     def send_head(k):
@@ -168,6 +195,7 @@
     def head_from(k):
         return remote(msg, heads.at[k], s_pre.at[k], r_pre.at[k], me, mt)
 
+    mark("send_head")
     span(me + 1, n_sp, lambda k: send_head(k).start())
 
     def columns_of(k):
@@ -175,18 +203,37 @@
 
     def send_wx(k):
         return remote(
-            wexit_hbm.at[:, columns_of(k)], wx.at[mt], s_wx.at[k], r_wx.at[mt], me, k)
+            wexit_hbm.at[quarter, columns_of(k)], wx.at[mt, quarter, :],
+            s_wx, r_wx.at[mt], me, k)
+
+    def quarter_of(j):
+        other = (x_part + j) % X_CHIPS
+        rows = pl.ds(pl.multiple_of(other * part, part), part)
+        return me - x_part + other, wx.at[:, rows, :], other
+
+    def send_quarter(j):
+        there, _, _ = quarter_of(j)
+        mine = wx.at[:, quarter, :]
+        return remote(mine, mine, s_wq, r_wq.at[x_part], there, mt)
 
     def send_dw(k):
         return remote(
-            down_hbm.at[0, :, columns_of(k)], dw.at[mt], s_dw.at[k], r_dw.at[mt], me, k)
-
+            down_hbm.at[0, :, columns_of(k)], dw.at[mt], s_dw, r_dw.at[mt], me, k)
+
+    def send_dw_to(d):
+        for c in range(CORES):
+            send_dw(chip(d) * CORES + c).start()
+
+    mark("send_wx")
     each(n_tp, mt, lambda k: send_wx(k).start())
-
-    sel, score = sel_ref[...], score_ref[...]
-    expert = iota((tok, n_sp), 1)
-    hit0 = (sel[:, 0:1] == expert).astype(F32)
-    hit1 = (sel[:, 1:2] == expert).astype(F32)
+    for d in away[:DW_EARLY]:
+        send_dw_to(d)
+
+    mark("routing")
+    sel, score = sel_ref[...].astype(F32), score_ref[...]
+    expert = iota((tok, n_sp), 1).astype(F32)
+    hit0 = (to_col(sel[0:1]) == expert).astype(F32)
+    hit1 = (to_col(sel[1:2]) == expert).astype(F32)
     hits = (hit0 + hit1).astype(BF16)
     below = (iota((tok, tok), 1) < iota((tok, tok), 0)).astype(F32).astype(BF16)
     rank = jnp.dot(below, hits, preferred_element_type=F32).astype(BF16)
@@ -198,14 +245,16 @@
     place = jnp.bitwise_and(iota((tok, slots), 1), cap - 1).astype(F32)
     picked = (hits_x > 0.5) & (rank_x == place)
     disp[...] = picked.astype(F32).astype(BF16)
-    both = score[:, 0:1] + score[:, 1:2]
-    share = jnp.where(hit0_x > 0.5, score[:, 0:1] / both, score[:, 1:2] / both)
+    both = score[0:1] + score[1:2]
+    share = jnp.where(hit0_x > 0.5, to_col(score[0:1] / both), to_col(score[1:2] / both))
     share = jnp.where(picked, share, 0.0)
     high = share.astype(BF16)
     whi[...] = high
     wlo[...] = (share - high.astype(F32)).astype(BF16)
 
+    mark("wait_head")
     span(0, me, lambda k: head_from(k).wait_recv())
+    mark("enter")
     w_re, w_im = cos, sin
     shift = 1
     while shift < tok:
@@ -229,21 +278,42 @@
             - jnp.dot(c_im, cum_i[g], precision=HIGH, preferred_element_type=F32))
         mx[mt, g * lanes:(g + 1) * lanes, :] = jax.nn.gelu(value).astype(BF16)
 
-    def send_mx(k):
-        return remote(mx.at[mt], mx.at[mt], s_mx.at[k], r_mx.at[mt], me, k)
-
-    each(n_tp, mt, lambda k: send_mx(k).start())
-    each(n_tp, mt, lambda k: send_dw(k).start())
-
-    def wait_tp(buf, sems):
-        each(n_tp, mt, lambda k: remote(
-            buf.at[k], buf.at[k], sems.at[k], sems.at[k], me, k).wait_recv())
-
+    def send_mx(owner, tp):
+        return remote(mx.at[owner], mx.at[owner], s_mx, r_mx.at[owner], me, tp)
+
+    mark("send_mx")
+    for d in away:
+        send_mx(mt, chip(d) * CORES + core).start()
+    send_mx(mt, twin).start()
+
+    def got(dst, sem):
+        remote(dst, dst, s_mx, sem, me, twin).wait_recv()
+
+    mark("wait_quarter")
+    local[2].wait()
+    each(n_tp, mt, lambda k: got(wx.at[k, quarter, :], r_wx.at[k]))
+    for j in range(1, X_CHIPS):
+        send_quarter(j).start()
+    for d in away[DW_EARLY:]:
+        send_dw_to(d)
+    send_dw(twin).start()
+
+    mark("relay_mx")
     local[0].wait()
     local[1].wait()
-    local[2].wait()
-    wait_tp(wx, r_wx)
-    wait_tp(mx, r_mx)
+    for d in away:
+        owner = chip(-d) * CORES + core
+        got(mx.at[owner], r_mx.at[owner])
+        send_mx(owner, twin).start()
+    mark("wait_wq")
+    for j in range(1, X_CHIPS):
+        _, dst, other = quarter_of(j)
+        got(dst, r_wq.at[other])
+    mark("wait_mx")
+    for d in [0] + away:
+        owner = chip(-d) * CORES + (1 - core)
+        got(mx.at[owner], r_mx.at[owner])
+    mark("project")
     projected = lax.dot_general(
         mx[...].reshape(n_tp * chan, tok), wx[...].reshape(n_tp * chan, d_local),
         (((0,), (0,)), ((), ())), preferred_element_type=F32).astype(BF16)
@@ -264,35 +334,42 @@
 
     def send_rows(k):
         return remote(
-            xs.at[k], g_buf.at[mt, rows_of(me), :], s_dis.at[k], r_dis.at[me], k, mt)
-
+            xs.at[k], g_buf.at[mt, rows_of(me), :], s_dis, r_dis.at[me], k, mt)
+
+    mark("send_rows")
     each(n_sp, me, lambda k: send_rows(k).start())
     own_rows = pltpu.make_async_copy(xs.at[me], g_buf.at[mt, rows_of(me), :], l_sem.at[6])
     own_rows.start()
 
+    one = pl.ds(0, 1)
+
     def send_ss(k):
-        return remote(ss.at[mt], ss.at[mt], s_ss.at[k], r_ss.at[mt], me, k)
+        mine = ss.at[mt, one, :]
+        return remote(mine, mine, s_ss, r_ss.at[mt], me, k)
 
     each(n_tp, mt, lambda k: send_ss(k).start())
-    wait_tp(ss, r_ss)
-    norm = lax.rsqrt(jnp.sum(ss[...], axis=0)[0:1, :] * (1.0 / width) + EPS)
-    norm_x = jnp.sum(disp[...].astype(F32) * to_col(norm), axis=0, keepdims=True)
-    for k in range(slots // 128):
-        inv[k] = jnp.broadcast_to(norm_x[:, k * 128:(k + 1) * 128], (8, 128))
 
     def tile_of(k):
         return (k * cap) // 128
 
     def send_inv(k):
         return remote(
-            inv.at[tile_of(k)], rinv.at[me], s_inv.at[k], r_inv.at[me], k, mt)
-
-    each(n_sp, me, lambda k: send_inv(k).start())
-    rinv[me] = inv[tile_of(me)]
+            inv.at[tile_of(k), one, :], rinv.at[me, one, :], s_inv, r_inv.at[me], k, mt)
+
+    def norm_factors():
+        mark("wait_ss")
+        each(n_tp, mt, lambda k: got(ss.at[k, one, :], r_ss.at[k]))
+        mark("norm")
+        norm = lax.rsqrt(jnp.sum(ss[...], axis=0)[0:1, :] * (1.0 / width) + EPS)
+        norm_x = jnp.sum(disp[...].astype(F32) * to_col(norm), axis=0, keepdims=True)
+        for k in range(slots // 128):
+            inv[k] = jnp.broadcast_to(norm_x[:, k * 128:(k + 1) * 128], (8, 128))
+        each(n_sp, me, lambda k: send_inv(k).start())
+        rinv[me] = inv[tile_of(me)]
 
     def inv_of(q):
-        part = rinv[q * sp_q:(q + 1) * sp_q]
-        full = jnp.concatenate([part] * (cap // 8), axis=1).reshape(rows_q, 128)
+        part = rinv[q * sp_q:(q + 1) * sp_q][:, 0:1, :]
+        full = jnp.broadcast_to(part, (sp_q, cap, 128)).reshape(rows_q, 128)
         want = (me * cap) % 128 + jnp.bitwise_and(iota((rows_q, 128), 0), cap - 1)
         return jnp.sum(jnp.where(iota((rows_q, 128), 1) == want, full, 0.0), axis=1, keepdims=True)
 
@@ -302,56 +379,44 @@
 
     deepest = n_y // 2
 
-    def chip(k):
-        return lax.rem(y + k + n_y, n_y)
-
-    started = []
-
     def ring_hop(buf, send, recv, q, h):
         rows = pl.ds(q * rows_q, rows_q)
 
-        def push(owner, tp, slot):
-            copy = remote(
-                buf.at[owner, rows, :], buf.at[owner, rows, :],
-                send.at[slot, q], recv.at[owner, q], me, tp)
-            copy.start()
-            started.append(copy)
+        def push(owner, tp):
+            there = buf.at[owner, rows, :]
+            remote(there, there, send.at[q], recv.at[owner, q], me, tp).start()
 
         def arrived(owner):
-            remote(
-                buf.at[owner, rows, :], buf.at[owner, rows, :],
-                send.at[0, q], recv.at[owner, q], me, mt).wait_recv()
+            got(buf.at[owner, rows, :], recv.at[owner, q])
 
         right, left = hops(q)
         right_tp, left_tp = chip(1) * CORES + core, chip(-1) * CORES + core
         if h == 0:
-            push(mt, right_tp, 0)
-            push(mt, left_tp, 1)
-            push(mt, twin, 2)
+            push(mt, right_tp)
+            push(mt, left_tp)
+            push(mt, twin)
             return
         if h <= right:
             owner = chip(-h) * CORES + core
             arrived(owner)
             if h < right:
-                push(owner, right_tp, 3 * h)
-            push(owner, twin, 3 * h + 2)
+                push(owner, right_tp)
+            push(owner, twin)
         if h <= left:
             owner = chip(h) * CORES + core
             arrived(owner)
             if h < left:
-                push(owner, left_tp, 3 * h + 1)
-            push(owner, twin, 3 * (deepest + 1) + h)
-
-    def pairs(buf, send, recv, q, h, weights, target, deep):
+                push(owner, left_tp)
+            push(owner, twin)
+
+    def pairs(buf, recv, q, h, weights, target):
         rows = pl.ds(q * rows_q, rows_q)
         right, left = hops(q)
         owners = [0] if h == 0 else [-h] * (h <= right) + [h] * (h <= left)
         for k in owners:
             there = chip(k)
             other = there * CORES + (1 - core)
-            remote(
-                buf.at[other, rows, :], buf.at[other, rows, :],
-                send.at[0, q], recv.at[other, q], me, mt).wait_recv()
+            got(buf.at[other, rows, :], recv.at[other, q])
             both = jnp.concatenate(
                 [buf[there * CORES, rows, :], buf[there * CORES + 1, rows, :]], axis=1)
             part = jnp.dot(both, weights(there), preferred_element_type=F32)
@@ -369,7 +434,7 @@
 
     def send_back(k):
         return remote(
-            outb.at[rows_of(k), :], ret.at[rows_of(me), :], s_ret.at[k], r_ret.at[me], k, mt)
+            outb.at[rows_of(k), :], ret.at[rows_of(me), :], s_ret, r_ret.at[me], k, mt)
 
     own_back = pltpu.make_async_copy(
         outb.at[rows_of(me), :], ret.at[rows_of(me), :], l_sem.at[7])
@@ -378,23 +443,21 @@
         rows = slice(q * rows_q, (q + 1) * rows_q)
         first = deepest + 1
         if st == 0:
-            def got(k):
+            def arrival(k):
                 @pl.when(k != me)
                 def _():
-                    remote(
-                        xs.at[0], g_buf.at[mt, rows_of(k), :], s_dis.at[k], r_dis.at[k],
-                        me, mt).wait_recv()
+                    got(g_buf.at[mt, rows_of(k), :], r_dis.at[k])
 
                 @pl.when(k == me)
                 def _():
                     own_rows.wait()
-            span(q * sp_q, (q + 1) * sp_q, got)
+            span(q * sp_q, (q + 1) * sp_q, arrival)
             ring_hop(g_buf, s_g, r_g, q, 0)
         elif st <= deepest:
             ring_hop(g_buf, s_g, r_g, q, st)
-            pairs(g_buf, s_g, r_g, q, st - 1, gate_up, acc, None)
+            pairs(g_buf, r_g, q, st - 1, gate_up, acc)
         elif st == first:
-            pairs(g_buf, s_g, r_g, q, deepest, gate_up, acc, None)
+            pairs(g_buf, r_g, q, deepest, gate_up, acc)
             factor = inv_of(q)
             gate = acc[rows, 0:f_local] * factor
             wide = acc[rows, f_local:2 * f_local] * factor
@@ -402,9 +465,9 @@
             ring_hop(h_buf, s_h, r_h, q, 0)
         elif st <= first + deepest:
             ring_hop(h_buf, s_h, r_h, q, st - first)
-            pairs(h_buf, s_h, r_h, q, st - first - 1, down, oacc, None)
+            pairs(h_buf, r_h, q, st - first - 1, down, oacc)
         else:
-            pairs(h_buf, s_h, r_h, q, deepest, down, oacc, None)
+            pairs(h_buf, r_h, q, deepest, down, oacc)
             outb[rows, :] = oacc[rows, :].astype(BF16)
 
             def back(k):
@@ -418,38 +481,56 @@
             span(q * sp_q, (q + 1) * sp_q, back)
 
     last_stage = 2 * deepest + 2
-    order = sorted((st + SKEW * q, q, st) for q in range(CHUNKS) for st in range(last_stage + 1))
-    ready = {0: False, 1: False}
+    order = sorted(
+        (st + SKEW * q if st else -1, q, st) for q in range(CHUNKS) for st in range(last_stage + 1))
+    ready = [False] * 3
     for _, q, st in order:
         if st == 1 and not ready[0]:
             local[3].wait()
             local[4].wait()
             ready[0] = True
+        if st == 3 and not ready[2]:
+            norm_factors()
+            ready[2] = True
         if st == deepest + 1 and not ready[1]:
-            each(n_sp, me, lambda k: remote(
-                inv.at[0], rinv.at[k], s_inv.at[k], r_inv.at[k], me, mt).wait_recv())
+            mark("wait_inv")
+            each(n_sp, me, lambda k: got(rinv.at[k, one, :], r_inv.at[k]))
+            mark("wait_dw")
             local[5].wait()
-            wait_tp(dw, r_dw)
+            each(n_tp, mt, lambda k: got(dw.at[k], r_dw.at[k]))
             ready[1] = True
+        mark(f"stage#t={st + SKEW * q}#q={q}#st={st}")
         stage(q, st)
 
+    mark("wait_back")
     own_back.wait()
-    each(n_sp, me, lambda k: remote(
-        outb.at[rows_of(k), :], ret.at[rows_of(k), :], s_ret.at[k], r_ret.at[k],
-        me, mt).wait_recv())
+    each(n_sp, me, lambda k: got(ret.at[rows_of(k), :], r_ret.at[k]))
+    mark("combine")
     back = ret[...]
     out_ref[...] = (
         stream_s[...]
         + jnp.dot(whi[...], back, preferred_element_type=F32)
         + jnp.dot(wlo[...], back, preferred_element_type=F32)).astype(BF16)
 
+    mark("drain")
     span(me + 1, n_sp, lambda k: send_head(k).wait_send())
-    for fn in (send_wx, send_mx, send_dw, send_ss):
-        each(n_tp, mt, lambda k: fn(k).wait_send())
-    for fn in (send_rows, send_inv, send_back):
-        each(n_sp, me, lambda k: fn(k).wait_send())
-    for copy in started:
-        copy.wait_send()
+
+    def sent_all(view, sem):
+        remote(view, view, sem, sem, me, twin).wait_send()
+
+    sent_all(wx.at[pl.ds(0, n_tp - 1), quarter, :], s_wx)
+    sent_all(wx.at[:, pl.ds(0, part * (X_CHIPS - 1)), :], s_wq)
+    sent_all(mx.at[pl.ds(0, 2 * n_y - 1)], s_mx)
+    sent_all(dw.at[pl.ds(0, n_tp - 1)], s_dw)
+    sent_all(ss.at[pl.ds(0, n_tp - 1), one, :], s_ss)
+    sent_all(xs.at[pl.ds(0, n_sp - 1)], s_dis)
+    sent_all(rinv.at[pl.ds(0, n_sp - 1), one, :], s_inv)
+    sent_all(outb.at[pl.ds(0, (n_sp - 1) * cap), :], s_ret)
+    for q in range(CHUNKS):
+        rows = pl.ds(q * rows_q, rows_q)
+        sent_all(g_buf.at[pl.ds(0, 2 * n_y - 1), rows, :], s_g.at[q])
+        sent_all(h_buf.at[pl.ds(0, 2 * n_y - 1), rows, :], s_h.at[q])
+    mark(None)
 
 
 def per_device(
@@ -467,7 +548,6 @@
     f_local = specialist_valve_matrix.shape[2]
     cap = 2 * tok * selected_specialists.shape[1] // n_sp
     slots = n_sp * cap
-    deepest = n_tp // CORES // 2
     dims = (n_sp, n_tp, groups, states, lanes, tok, width, cap)
     vmem = pl.BlockSpec(memory_space=pltpu.VMEM)
     hbm = pl.BlockSpec(memory_space=pl.ANY)
@@ -500,11 +580,9 @@
         pltpu.VMEM((groups, states, tok), F32),
         dma((8,)),
         dma((n_sp,)), dma((n_sp,)),
-        dma((n_tp,)), dma((n_tp,)), dma((n_tp,)), dma((n_tp,)),
-        dma((n_tp,)), dma((n_tp,)), dma((n_tp,)), dma((n_tp,)),
-        dma((n_sp,)), dma((n_sp,)), dma((n_sp,)), dma((n_sp,)), dma((n_sp,)), dma((n_sp,)),
-        dma((4 * deepest + 4, CHUNKS)), dma((n_tp, CHUNKS)),
-        dma((4 * deepest + 4, CHUNKS)), dma((n_tp, CHUNKS)),
+        dma, dma((n_tp,)), dma, dma((X_CHIPS,)), dma, dma((n_tp,)), dma, dma((n_tp,)),
+        dma, dma((n_tp,)), dma, dma((n_sp,)), dma, dma((n_sp,)), dma, dma((n_sp,)),
+        dma((CHUNKS,)), dma((n_tp, CHUNKS)), dma((CHUNKS,)), dma((n_tp, CHUNKS)),
     ]
     return pl.pallas_call(
         functools.partial(mixer_kernel, dims),
@@ -516,9 +594,10 @@
             collective_id=0, has_side_effects=True, vmem_limit_bytes=60 * 1024 * 1024),
     )(
         lane_source_signal, spectral_damping_part, spectral_angular_part,
-        interval_exponent.reshape(1, groups), entry_matrix_inphase, entry_matrix_quadrature,
+        interval_exponent.reshape(1, groups), entry_matrix_inphase.transpose(0, 2, 1),
+        entry_matrix_quadrature.transpose(0, 2, 1),
         emission_inphase, emission_quadrature, lane_bypass_factor.reshape(1, chan),
-        spike_shrink_offset, selected_specialists, dispatcher_scores, lane_exit_matrix,
+        spike_shrink_offset, selected_specialists.T, dispatcher_scores.T, lane_exit_matrix,
         skipline_stream, specialist_scaling_vector.reshape(1, width),
         specialist_valve_matrix, specialist_widen_matrix, specialist_shrink_matrix,
     )

time: 126 us -> 98.7 us (0.78)
  Pallas kernels: 120 us -> 96.9 us
  local copies, waits for them, and re-layouts: 5.15 us -> 1.47 us
    pallas_call x1, Pallas kernels: 120 us -> 96.9 us  [per_device(): pl.pallas_call(functools.partial(mixer_kernel, dims), out_shape=jax.Shape...]
    unnamed x13 -> x1, local copies, waits for them, and re-layouts: 5.15 us -> 1.47 us
where the time goes in v2:
time: 98.7 us; the launch traced here: 98.4 us
  Pallas kernels  96.9 us (98%)
  local copies, waits for them, and re-layouts  1.47 us (1%)
    pallas_call x1, Pallas kernels, per_device(): pl.pallas_call(functools.partial(mixer_kernel, dims), out_shape=jax.Shape...  96.9 us

profile of v2, /device:TPU:1, one launch (start us, length us, event | category | flops | bytes accessed | tf_op | source)
XLA Modules:
  0.0 98.4 jit_solution(6821889529017069303)
XLA Ops:
  0.0 96.9 %shard_map.172 = bf16[128,256]{1,0:T(8,128)(2,1)} custom-call(bf16[64,128]{1,0:T(8,128)(2,1)} %u_ref.1, f32[4,64]{1,0:T(4,128)} %damp_ref.1, f32[4,64]{1,0:T(4,128)} %ang_ref.1, f32[1,4]{1,0:T(1,128)} %bitcast.12, f32[4,16,64]{2,1,0:T(8,128)} %bitcast.7, f32[4,16,64]{2,1,0:T(8,128)} %bitcast.8, f32[4,16,64]{2,1,0:T(8,128)} %cin_ref.1, f32[4,16,64]{2,1,0:T(8,128)} %cq_ref.1, ...), custom_call_target="tpu_custom_call" | custom-call | tf_op jit(solution)/shard_map/pallas_call | solution.py:587
  96.9 1.5 %copy.20 = bf16[128,256]{1,0:T(8,128)(2,1)} copy(bf16[128,256]{1,0:T(8,128)(2,1)} %shard_map.172) | data formatting | bytes 131072

commit v3 on v2

--- a/solution.py
+++ b/solution.py
@@ -16,7 +16,10 @@
 CHUNKS = 4
 SKEW = 0.5
 X_CHIPS = 4
-DW_EARLY = 2
+DW_EARLY, DW_MID = 4, 12
+PIECE = 32
+DW_SLOTS = ((2, 3), (3, 3), (0, 4), (1, 4), (2, 4), (3, 4), (0, 6), (1, 6))
+CHUNK_ORDER = (0, 1, 2, 3)
 
 
 def iota(shape, dim):
@@ -53,13 +56,15 @@
 
 def mixer_kernel(
     dims,
+    u_hbm, damp_hbm, ang_hbm, ie_hbm, ein_hbm, eq_hbm, cin_hbm, cq_hbm, byp_hbm, off_hbm,
+    sel_hbm, score_hbm, wexit_hbm, skip_hbm, gain_hbm, gate_hbm, up_hbm, down_hbm,
+    out_ref,
     u_ref, damp_ref, ang_ref, ie_ref, ein_ref, eq_ref, cin_ref, cq_ref, byp_ref, off_ref,
-    sel_ref, score_ref, wexit_hbm, skip_hbm, gain_hbm, gate_hbm, up_hbm, down_hbm,
-    out_ref,
-    msg, heads, wx, mx, dw, gu, skip, gain, ss, inv, rinv, disp, whi, wlo,
+    sel_ref, score_ref,
+    msg, heads, wx, mx, dw, gu, skip, gain, squares, disp, whi, wlo,
     xs, g_buf, h_buf, acc, oacc, outb, ret, stream_s, loc_r, cum_r, cum_i,
-    l_sem, s_pre, r_pre, s_wx, r_wx, s_wq, r_wq, s_mx, r_mx, s_dw, r_dw, s_ss, r_ss,
-    s_inv, r_inv, s_dis, r_dis, s_ret, r_ret, s_g, r_g, s_h, r_h,
+    i_sem, l_sem, s_pre, r_pre, s_wx, r_wx, s_wq, r_wq, s_mx, r_mx, s_dw, r_dw,
+    s_dis, r_dis, s_ret, r_ret, *ring_sems,
 ):
     n_sp, n_tp, groups, states, lanes, tok, width, cap = dims
     n_y = n_tp // CORES
@@ -75,13 +80,35 @@
     away = [k for d in range(1, n_y // 2 + 1) for k in ((d, -d) if 2 * d < n_y else (d,))]
 
     def chip(k):
-        return lax.rem(y + k + n_y, n_y)
+        return around(y + k, n_y)
+
+    def around(value, count):
+        if count & (count - 1):
+            return lax.rem(value + count, count)
+        return jnp.bitwise_and(value, count - 1)
 
     def each(count, mine, fn):
-        def step(j, carry):
-            fn(lax.rem(mine + j, count))
-            return carry
-        lax.fori_loop(1, count, step, 0)
+        for j in range(1, count):
+            fn(around(mine + j, count))
+
+    n_z = n_sp // X_CHIPS
+    near = sorted(
+        ((dz, dx) for dz in range(-((n_z - 1) // 2), n_z // 2 + 1)
+         for dx in range(-((X_CHIPS - 1) // 2), X_CHIPS // 2 + 1)),
+        key=lambda o: (-(abs(o[0]) + abs(o[1])), -abs(o[0]), o))
+
+    def at_offset(dz, dx):
+        return around(me // X_CHIPS + dz, n_z) * X_CHIPS + around(x_part + dx, X_CHIPS)
+
+    def place_at(dz, dx):
+        back = [
+            k for k, (a, b) in enumerate(near)
+            if (a + dz) % n_z == 0 and (b + dx) % X_CHIPS == 0]
+        return back[0]
+
+    def far_first(fn):
+        for dz, dx in near[:-1]:
+            fn(dz, dx)
 
     def span(lo, hi, fn):
         def step(j, carry):
@@ -103,12 +130,25 @@
             scope.append(jax.named_scope(name))
             scope[-1].__enter__()
 
+    small = [
+        pltpu.make_async_copy(src, dst, i_sem.at[k])
+        for k, (src, dst) in enumerate((
+            (ie_hbm, ie_ref), (damp_hbm, damp_ref), (ang_hbm, ang_ref), (off_hbm, off_ref),
+            (u_hbm, u_ref), (ein_hbm, ein_ref), (eq_hbm, eq_ref), (cin_hbm, cin_ref),
+            (cq_hbm, cq_ref), (byp_hbm, byp_ref), (sel_hbm, sel_ref), (score_hbm, score_ref)))
+    ]
+    for copy in small:
+        copy.start()
+
     heads[...] = jnp.zeros_like(heads)
     barrier = pltpu.get_barrier_semaphore()
-    each(n_sp, me, lambda k: pl.semaphore_signal(
-        barrier, inc=1, device_id=(k, mt), device_id_type=MESH))
-    each(n_tp, mt, lambda k: pl.semaphore_signal(
-        barrier, inc=1, device_id=(me, k), device_id_type=MESH))
+    far_first(lambda dz, dx: pl.semaphore_signal(
+        barrier, inc=1, device_id=(at_offset(dz, dx), mt), device_id_type=MESH))
+    for d in away[::-1]:
+        for c in range(CORES):
+            pl.semaphore_signal(
+                barrier, inc=1, device_id=(me, chip(d) * CORES + c), device_id_type=MESH)
+    pl.semaphore_signal(barrier, inc=1, device_id=(me, twin), device_id_type=MESH)
 
     mark("local_copies")
     own_cols = pl.ds(pl.multiple_of(mt * d_local, d_local), d_local)
@@ -117,7 +157,7 @@
     quarter = pl.ds(pl.multiple_of(x_part * part, part), part)
     local = [
         pltpu.make_async_copy(skip_hbm.at[:, own_cols], skip, l_sem.at[0]),
-        pltpu.make_async_copy(gain_hbm.at[:, own_cols], gain, l_sem.at[1]),
+        pltpu.make_async_copy(gain_hbm, gain, l_sem.at[1]),
         pltpu.make_async_copy(
             wexit_hbm.at[quarter, own_cols], wx.at[mt, quarter, :], l_sem.at[2]),
         pltpu.make_async_copy(gate_hbm.at[0], gu.at[:, pl.ds(0, f_local)], l_sem.at[3]),
@@ -128,6 +168,8 @@
         copy.start()
 
     mark("state")
+    for copy in small:
+        copy.wait()
     step_size = jnp.exp(to_col(ie_ref[...]))
     damp, ang = damp_ref[...], ang_ref[...]
     rate, angle = damp * step_size, ang * step_size
@@ -220,14 +262,22 @@
         return remote(
             down_hbm.at[0, :, columns_of(k)], dw.at[mt], s_dw, r_dw.at[mt], me, k)
 
-    def send_dw_to(d):
-        for c in range(CORES):
+    def send_piece(d, c, k):
+        there = chip(d) * CORES + c
+        rows = pl.ds(k * PIECE, PIECE)
+        return remote(
+            down_hbm.at[0, rows, columns_of(there)], dw.at[mt, rows, :],
+            s_dw, r_dw.at[mt], me, there)
+
+    targets = [(d, c) for d in away for c in range(CORES)]
+
+    def send_dw_to(those):
+        for d, c in those:
             send_dw(chip(d) * CORES + c).start()
 
     mark("send_wx")
     each(n_tp, mt, lambda k: send_wx(k).start())
-    for d in away[:DW_EARLY]:
-        send_dw_to(d)
+    send_dw_to(targets[:DW_EARLY])
 
     mark("routing")
     sel, score = sel_ref[...].astype(F32), score_ref[...]
@@ -294,13 +344,11 @@
     each(n_tp, mt, lambda k: got(wx.at[k, quarter, :], r_wx.at[k]))
     for j in range(1, X_CHIPS):
         send_quarter(j).start()
-    for d in away[DW_EARLY:]:
-        send_dw_to(d)
+    send_dw_to(targets[DW_EARLY:DW_MID])
     send_dw(twin).start()
 
     mark("relay_mx")
     local[0].wait()
-    local[1].wait()
     for d in away:
         owner = chip(-d) * CORES + core
         got(mx.at[owner], r_mx.at[owner])
@@ -320,188 +368,193 @@
     stream = (skip[...].astype(F32) + projected.astype(F32)).astype(BF16)
     stream_f = stream.astype(F32)
     stream_s[...] = stream_f
-    squares = to_row(jnp.sum(stream_f * stream_f, axis=1, keepdims=True))
-    ss[mt] = jnp.broadcast_to(squares, (8, tok))
-
-    scaled = (stream_f * gain[...]).astype(BF16)
+
     sent = lax.dot_general(
-        disp[...], scaled, (((0,), (0,)), ((), ())),
+        disp[...], stream, (((0,), (0,)), ((), ())),
         preferred_element_type=F32).astype(BF16).reshape(n_sp, cap, d_local)
     xs[...] = sent
 
     def rows_of(k):
-        return pl.ds(pl.multiple_of(k * cap, cap), cap)
-
-    def send_rows(k):
+        start = k * cap
+        return pl.ds(start if isinstance(k, int) else pl.multiple_of(start, cap), cap)
+
+    own_place = n_sp - 1
+
+    def send_rows(dz, dx):
+        k, place = at_offset(dz, dx), place_at(dz, dx)
         return remote(
-            xs.at[k], g_buf.at[mt, rows_of(me), :], s_dis, r_dis.at[me], k, mt)
+            xs.at[k], g_buf.at[mt, rows_of(place), :], s_dis, r_dis.at[place], k, mt)
 
     mark("send_rows")
-    each(n_sp, me, lambda k: send_rows(k).start())
-    own_rows = pltpu.make_async_copy(xs.at[me], g_buf.at[mt, rows_of(me), :], l_sem.at[6])
+    far_first(lambda dz, dx: send_rows(dz, dx).start())
+    own_rows = pltpu.make_async_copy(
+        xs.at[me], g_buf.at[mt, rows_of(own_place), :], l_sem.at[6])
     own_rows.start()
 
-    one = pl.ds(0, 1)
-
-    def send_ss(k):
-        mine = ss.at[mt, one, :]
-        return remote(mine, mine, s_ss, r_ss.at[mt], me, k)
-
-    each(n_tp, mt, lambda k: send_ss(k).start())
-
-    def tile_of(k):
-        return (k * cap) // 128
-
-    def send_inv(k):
-        return remote(
-            inv.at[tile_of(k), one, :], rinv.at[me, one, :], s_inv, r_inv.at[me], k, mt)
-
-    def norm_factors():
-        mark("wait_ss")
-        each(n_tp, mt, lambda k: got(ss.at[k, one, :], r_ss.at[k]))
-        mark("norm")
-        norm = lax.rsqrt(jnp.sum(ss[...], axis=0)[0:1, :] * (1.0 / width) + EPS)
-        norm_x = jnp.sum(disp[...].astype(F32) * to_col(norm), axis=0, keepdims=True)
-        for k in range(slots // 128):
-            inv[k] = jnp.broadcast_to(norm_x[:, k * 128:(k + 1) * 128], (8, 128))
-        each(n_sp, me, lambda k: send_inv(k).start())
-        rinv[me] = inv[tile_of(me)]
-
-    def inv_of(q):
-        part = rinv[q * sp_q:(q + 1) * sp_q][:, 0:1, :]
-        full = jnp.broadcast_to(part, (sp_q, cap, 128)).reshape(rows_q, 128)
-        want = (me * cap) % 128 + jnp.bitwise_and(iota((rows_q, 128), 0), cap - 1)
-        return jnp.sum(jnp.where(iota((rows_q, 128), 1) == want, full, 0.0), axis=1, keepdims=True)
-
-    def hops(q):
-        far, near = n_y // 2, n_y - 1 - n_y // 2
-        return (far, near) if q % 2 == 0 else (near, far)
-
     deepest = n_y // 2
 
-    def ring_hop(buf, send, recv, q, h):
-        rows = pl.ds(q * rows_q, rows_q)
-
-        def push(owner, tp):
-            there = buf.at[owner, rows, :]
-            remote(there, there, send.at[q], recv.at[owner, q], me, tp).start()
-
-        def arrived(owner):
-            got(buf.at[owner, rows, :], recv.at[owner, q])
-
-        right, left = hops(q)
-        right_tp, left_tp = chip(1) * CORES + core, chip(-1) * CORES + core
+    way = 1 - 2 * core
+    onward = around(y + way, n_y) * CORES + core
+
+    def rows_in(q):
+        return pl.ds(q * rows_q, rows_q)
+
+    def half_in(q, side):
+        size = rows_q // CORES
+        return pl.ds(pl.multiple_of(q * rows_q + side * size, size), size)
+
+    def chip_rows(buf, there, rows):
+        return buf.at[pl.ds(there * CORES, CORES), rows, :]
+
+    def ring_hop(buf, sems, q, h):
+        send, one, ring, handed = sems
+
+        def push(view, sem, tp):
+            remote(view, view, send.at[q], sem, me, tp).start()
+
         if h == 0:
-            push(mt, right_tp)
-            push(mt, left_tp)
-            push(mt, twin)
+            for tp in (chip(1) * CORES, chip(-1) * CORES + 1, twin):
+                push(buf.at[mt, rows_in(q), :], one.at[mt, q], tp)
             return
-        if h <= right:
-            owner = chip(-h) * CORES + core
-            arrived(owner)
-            if h < right:
-                push(owner, right_tp)
-            push(owner, twin)
-        if h <= left:
-            owner = chip(h) * CORES + core
-            arrived(owner)
-            if h < left:
-                push(owner, left_tp)
-            push(owner, twin)
-
-    def pairs(buf, recv, q, h, weights, target):
-        rows = pl.ds(q * rows_q, rows_q)
-        right, left = hops(q)
-        owners = [0] if h == 0 else [-h] * (h <= right) + [h] * (h <= left)
-        for k in owners:
-            there = chip(k)
-            other = there * CORES + (1 - core)
-            got(buf.at[other, rows, :], recv.at[other, q])
+        there = around(y - way * h, n_y)
+        view = chip_rows(buf, there, rows_in(q) if h < deepest else half_in(q, core))
+        if h == 1:
+            for c in range(CORES):
+                owner = there * CORES + c
+                got(buf.at[owner, rows_in(q), :], one.at[owner, q])
+        else:
+            got(view, ring.at[there, q])
+        if h < deepest:
+            rows = rows_in(q) if h < deepest - 1 else half_in(q, core)
+            push(chip_rows(buf, there, rows), ring.at[there, q], onward)
+        push(view, handed.at[there, q], twin)
+
+    def normed(both, there, rows, fresh):
+        depth = CORES * d_local
+        full = both.astype(F32)
+        square = full * full
+        total = square[:, 0:128]
+        for k in range(1, depth // 128):
+            total = total + square[:, k * 128:(k + 1) * 128]
+        squares[rows, :] = total if fresh else squares[rows, :] + total
+        gains = gain[:, pl.ds(pl.multiple_of(there * depth, depth), depth)]
+        return (full * gains).astype(BF16)
+
+    def pairs(buf, sems, q, h, weights, target, need=None):
+        _, one, _, handed = sems
+        rows = rows_in(q)
+
+        def multiply(there):
             both = jnp.concatenate(
                 [buf[there * CORES, rows, :], buf[there * CORES + 1, rows, :]], axis=1)
+            if need is None:
+                both = normed(both, there, rows, h == 0)
             part = jnp.dot(both, weights(there), preferred_element_type=F32)
             if h == 0:
                 target[rows, :] = part
             else:
                 target[rows, :] += part
 
+        if need is not None:
+            need(h)
+        other = around(y + way * h, n_y)
+        if h == 0:
+            got(buf.at[twin, rows, :], one.at[twin, q])
+        elif h < deepest:
+            multiply(around(y - way * h, n_y))
+            got(chip_rows(buf, other, rows), handed.at[other, q])
+        else:
+            got(chip_rows(buf, other, half_in(q, 1 - core)), handed.at[other, q])
+        multiply(other)
+
     def gate_up(there):
         depth = CORES * d_local
         return gu[pl.ds(pl.multiple_of(there * depth, depth), depth), :]
 
+    def down_here(k):
+        if k == 0:
+            local[5].wait()
+            got(dw.at[twin], r_dw.at[twin])
+        else:
+            for d in (k, -k) if 2 * k < n_y else (k,):
+                for c in range(CORES):
+                    owner = chip(d) * CORES + c
+                    got(dw.at[owner], r_dw.at[owner])
+
     def down(there):
         return jnp.concatenate([dw[there * CORES], dw[there * CORES + 1]], axis=0)
 
-    def send_back(k):
+    def send_back(place):
+        k = at_offset(*near[place])
         return remote(
-            outb.at[rows_of(k), :], ret.at[rows_of(me), :], s_ret, r_ret.at[me], k, mt)
+            outb.at[rows_of(place), :], ret.at[rows_of(me), :], s_ret, r_ret.at[me], k, mt)
 
     own_back = pltpu.make_async_copy(
-        outb.at[rows_of(me), :], ret.at[rows_of(me), :], l_sem.at[7])
-
-    def stage(q, st):
+        outb.at[rows_of(own_place), :], ret.at[rows_of(me), :], l_sem.at[7])
+
+    seen = set()
+    g_sems, h_sems = ring_sems[:4], ring_sems[4:]
+
+    def stage(r, q, st):
         rows = slice(q * rows_q, (q + 1) * rows_q)
         first = deepest + 1
+
+        def need(k):
+            if k not in seen:
+                seen.add(k)
+                down_here(k)
+
         if st == 0:
-            def arrival(k):
-                @pl.when(k != me)
-                def _():
-                    got(g_buf.at[mt, rows_of(k), :], r_dis.at[k])
-
-                @pl.when(k == me)
-                def _():
+            for place in range(q * sp_q, (q + 1) * sp_q):
+                if place == own_place:
                     own_rows.wait()
-            span(q * sp_q, (q + 1) * sp_q, arrival)
-            ring_hop(g_buf, s_g, r_g, q, 0)
+                else:
+                    got(g_buf.at[mt, rows_of(place), :], r_dis.at[place])
+            ring_hop(g_buf, g_sems, q, 0)
         elif st <= deepest:
-            ring_hop(g_buf, s_g, r_g, q, st)
-            pairs(g_buf, r_g, q, st - 1, gate_up, acc)
+            ring_hop(g_buf, g_sems, q, st)
+            pairs(g_buf, g_sems, q, st - 1, gate_up, acc)
         elif st == first:
-            pairs(g_buf, r_g, q, deepest, gate_up, acc)
-            factor = inv_of(q)
+            pairs(g_buf, g_sems, q, deepest, gate_up, acc)
+            mean = jnp.sum(squares[rows, :], axis=1, keepdims=True) * (1.0 / width)
+            factor = lax.rsqrt(mean + EPS)
             gate = acc[rows, 0:f_local] * factor
             wide = acc[rows, f_local:2 * f_local] * factor
             h_buf[mt, rows, :] = (jax.nn.silu(gate) * wide).astype(BF16)
-            ring_hop(h_buf, s_h, r_h, q, 0)
+            ring_hop(h_buf, h_sems, q, 0)
         elif st <= first + deepest:
-            ring_hop(h_buf, s_h, r_h, q, st - first)
-            pairs(h_buf, r_h, q, st - first - 1, down, oacc)
+            ring_hop(h_buf, h_sems, q, st - first)
+            pairs(h_buf, h_sems, q, st - first - 1, down, oacc, need)
         else:
-            pairs(h_buf, r_h, q, deepest, down, oacc)
+            pairs(h_buf, h_sems, q, deepest, down, oacc, need)
             outb[rows, :] = oacc[rows, :].astype(BF16)
 
-            def back(k):
-                @pl.when(k != me)
-                def _():
-                    send_back(k).start()
-
-                @pl.when(k == me)
-                def _():
+            for place in range(q * sp_q, (q + 1) * sp_q):
+                if place == own_place:
                     own_back.start()
-            span(q * sp_q, (q + 1) * sp_q, back)
+                else:
+                    send_back(place).start()
 
     last_stage = 2 * deepest + 2
+    pieces = [
+        (d, c, k) for d, c in targets[DW_MID:] for k in range(f_local // PIECE)]
     order = sorted(
-        (st + SKEW * q if st else -1, q, st) for q in range(CHUNKS) for st in range(last_stage + 1))
-    ready = [False] * 3
-    for _, q, st in order:
-        if st == 1 and not ready[0]:
+        (st + SKEW * r if st else -1, r, q, st)
+        for r, q in enumerate(CHUNK_ORDER) for st in range(last_stage + 1))
+    for now, (_, r, q, st) in enumerate(order):
+        if st == 1 and r == 0:
+            mark("wait_small")
+            local[1].wait()
             local[3].wait()
             local[4].wait()
-            ready[0] = True
-        if st == 3 and not ready[2]:
-            norm_factors()
-            ready[2] = True
-        if st == deepest + 1 and not ready[1]:
-            mark("wait_inv")
-            each(n_sp, me, lambda k: got(rinv.at[k, one, :], r_inv.at[k]))
-            mark("wait_dw")
-            local[5].wait()
-            each(n_tp, mt, lambda k: got(dw.at[k], r_dw.at[k]))
-            ready[1] = True
-        mark(f"stage#t={st + SKEW * q}#q={q}#st={st}")
-        stage(q, st)
-
+            span(me + 1, n_sp, lambda k: send_head(k).wait_send())
+        mark(f"stage#n={now}#r={r}#st={st}")
+        stage(r, q, st)
+        for d, c, k in pieces[:DW_SLOTS.count((r, st))]:
+            send_piece(d, c, k).start()
+        del pieces[:DW_SLOTS.count((r, st))]
+
+    assert not pieces
     mark("wait_back")
     own_back.wait()
     each(n_sp, me, lambda k: got(ret.at[rows_of(k), :], r_ret.at[k]))
@@ -513,7 +566,6 @@
         + jnp.dot(wlo[...], back, preferred_element_type=F32)).astype(BF16)
 
     mark("drain")
-    span(me + 1, n_sp, lambda k: send_head(k).wait_send())
 
     def sent_all(view, sem):
         remote(view, view, sem, sem, me, twin).wait_send()
@@ -522,14 +574,12 @@
     sent_all(wx.at[:, pl.ds(0, part * (X_CHIPS - 1)), :], s_wq)
     sent_all(mx.at[pl.ds(0, 2 * n_y - 1)], s_mx)
     sent_all(dw.at[pl.ds(0, n_tp - 1)], s_dw)
-    sent_all(ss.at[pl.ds(0, n_tp - 1), one, :], s_ss)
     sent_all(xs.at[pl.ds(0, n_sp - 1)], s_dis)
-    sent_all(rinv.at[pl.ds(0, n_sp - 1), one, :], s_inv)
     sent_all(outb.at[pl.ds(0, (n_sp - 1) * cap), :], s_ret)
     for q in range(CHUNKS):
         rows = pl.ds(q * rows_q, rows_q)
-        sent_all(g_buf.at[pl.ds(0, 2 * n_y - 1), rows, :], s_g.at[q])
-        sent_all(h_buf.at[pl.ds(0, 2 * n_y - 1), rows, :], s_h.at[q])
+        sent_all(g_buf.at[pl.ds(0, 2 * n_y - 1), rows, :], g_sems[0].at[q])
+        sent_all(h_buf.at[pl.ds(0, 2 * n_y - 1), rows, :], h_sems[0].at[q])
     mark(None)
 
 
@@ -550,9 +600,18 @@
     slots = n_sp * cap
     dims = (n_sp, n_tp, groups, states, lanes, tok, width, cap)
     vmem = pl.BlockSpec(memory_space=pltpu.VMEM)
+    operands = (
+        lane_source_signal, spectral_damping_part, spectral_angular_part,
+        interval_exponent.reshape(1, groups), entry_matrix_inphase.transpose(0, 2, 1),
+        entry_matrix_quadrature.transpose(0, 2, 1),
+        emission_inphase, emission_quadrature, lane_bypass_factor.reshape(1, chan),
+        spike_shrink_offset, selected_specialists.T, dispatcher_scores.T, lane_exit_matrix,
+        skipline_stream, specialist_scaling_vector.reshape(1, width),
+        specialist_valve_matrix, specialist_widen_matrix, specialist_shrink_matrix,
+    )
     hbm = pl.BlockSpec(memory_space=pl.ANY)
     dma = pltpu.SemaphoreType.DMA
-    scratch = [
+    scratch = [pltpu.VMEM(a.shape, a.dtype) for a in operands[:12]] + [
         pltpu.VMEM((8, 128), F32),
         pltpu.VMEM((n_sp, 8, 128), F32),
         pltpu.VMEM((n_tp, chan, d_local), BF16),
@@ -560,10 +619,8 @@
         pltpu.VMEM((n_tp, f_local, d_local), BF16),
         pltpu.VMEM((width, 2 * f_local), BF16),
         pltpu.VMEM((tok, d_local), BF16),
-        pltpu.VMEM((1, d_local), F32),
-        pltpu.VMEM((n_tp, 8, tok), F32),
-        pltpu.VMEM((slots // 128, 8, 128), F32),
-        pltpu.VMEM((n_sp, 8, 128), F32),
+        pltpu.VMEM((1, width), F32),
+        pltpu.VMEM((slots, 128), F32),
         pltpu.VMEM((tok, slots), BF16),
         pltpu.VMEM((tok, slots), BF16),
         pltpu.VMEM((tok, slots), BF16),
@@ -578,29 +635,23 @@
         pltpu.VMEM((groups, lanes, tok), F32),
         pltpu.VMEM((groups, states, tok), F32),
         pltpu.VMEM((groups, states, tok), F32),
-        dma((8,)),
+        dma((12,)), dma((8,)),
         dma((n_sp,)), dma((n_sp,)),
         dma, dma((n_tp,)), dma, dma((X_CHIPS,)), dma, dma((n_tp,)), dma, dma((n_tp,)),
-        dma, dma((n_tp,)), dma, dma((n_sp,)), dma, dma((n_sp,)), dma, dma((n_sp,)),
-        dma((CHUNKS,)), dma((n_tp, CHUNKS)), dma((CHUNKS,)), dma((n_tp, CHUNKS)),
+        dma, dma((n_sp,)), dma, dma((n_sp,)),
+    ] + 2 * [
+        dma((CHUNKS,)), dma((n_tp, CHUNKS)),
+        dma((n_tp // CORES, CHUNKS)), dma((n_tp // CORES, CHUNKS)),
     ]
     return pl.pallas_call(
         functools.partial(mixer_kernel, dims),
         out_shape=jax.ShapeDtypeStruct((tok, d_local), BF16),
-        in_specs=[vmem] * 12 + [hbm] * 6,
+        in_specs=[hbm] * 18,
         out_specs=vmem,
         scratch_shapes=scratch,
         compiler_params=pltpu.CompilerParams(
             collective_id=0, has_side_effects=True, vmem_limit_bytes=60 * 1024 * 1024),
-    )(
-        lane_source_signal, spectral_damping_part, spectral_angular_part,
-        interval_exponent.reshape(1, groups), entry_matrix_inphase.transpose(0, 2, 1),
-        entry_matrix_quadrature.transpose(0, 2, 1),
-        emission_inphase, emission_quadrature, lane_bypass_factor.reshape(1, chan),
-        spike_shrink_offset, selected_specialists.T, dispatcher_scores.T, lane_exit_matrix,
-        skipline_stream, specialist_scaling_vector.reshape(1, width),
-        specialist_valve_matrix, specialist_widen_matrix, specialist_shrink_matrix,
-    )
+    )(*operands)
 
 
 def solution(mesh):

time: 98.7 us -> 96.6 us (0.979)
  Pallas kernels: 96.9 us -> 94.9 us
    pallas_call x1, Pallas kernels: 96.9 us -> 94.9 us  [per_device(): pl.pallas_call(functools.partial(mixer_kernel, dims), out_shape=jax.Shape...]
where the time goes in v3:
time: 96.6 us; the launch traced here: 96.4 us
  Pallas kernels  94.9 us (98%)
  local copies, waits for them, and re-layouts  1.47 us (2%)
    pallas_call x1, Pallas kernels, per_device(): pl.pallas_call(functools.partial(mixer_kernel, dims), out_shape=jax.Shape...  94.9 us

profile of v3, /device:TPU:1, one launch (start us, length us, event | category | flops | bytes accessed | tf_op | source)
XLA Modules:
  0.0 96.4 jit_solution(16872539206645160131)
XLA Ops:
  0.0 94.9 %shard_map.172 = bf16[128,256]{1,0:T(8,128)(2,1)} custom-call(bf16[64,128]{1,0:T(8,128)(2,1)} %u_hbm.1, f32[4,64]{1,0:T(4,128)} %damp_hbm.1, f32[4,64]{1,0:T(4,128)} %ang_hbm.1, f32[1,4]{1,0:T(1,128)} %bitcast.12, f32[4,16,64]{2,1,0:T(8,128)} %bitcast.7, f32[4,16,64]{2,1,0:T(8,128)} %bitcast.8, f32[4,16,64]{2,1,0:T(8,128)} %cin_hbm.1, f32[4,16,64]{2,1,0:T(8,128)} %cq_hbm.1, ...), custom_call_target="tpu_custom_call" | custom-call | tf_op jit(solution)/shard_map/pallas_call | solution.py:646
  94.9 1.5 %copy.20 = bf16[128,256]{1,0:T(8,128)(2,1)} copy(bf16[128,256]{1,0:T(8,128)(2,1)} %shard_map.172) | data formatting | bytes 131072

commit v4 on v3

--- a/solution.py
+++ b/solution.py
@@ -19,6 +19,7 @@
 DW_EARLY, DW_MID = 4, 12
 PIECE = 32
 DW_SLOTS = ((2, 3), (3, 3), (0, 4), (1, 4), (2, 4), (3, 4), (0, 6), (1, 6))
+GROUP_SETS = ((0, 1, 2, 3),)
 CHUNK_ORDER = (0, 1, 2, 3)
 
 
@@ -130,6 +131,16 @@
             scope.append(jax.named_scope(name))
             scope[-1].__enter__()
 
+    heads[...] = jnp.zeros_like(heads)
+    barrier = pltpu.get_barrier_semaphore()
+    far_first(lambda dz, dx: pl.semaphore_signal(
+        barrier, inc=1, device_id=(at_offset(dz, dx), mt), device_id_type=MESH))
+    for d in away[::-1]:
+        for c in range(CORES):
+            pl.semaphore_signal(
+                barrier, inc=1, device_id=(me, chip(d) * CORES + c), device_id_type=MESH)
+    pl.semaphore_signal(barrier, inc=1, device_id=(me, twin), device_id_type=MESH)
+
     small = [
         pltpu.make_async_copy(src, dst, i_sem.at[k])
         for k, (src, dst) in enumerate((
@@ -139,16 +150,6 @@
     ]
     for copy in small:
         copy.start()
-
-    heads[...] = jnp.zeros_like(heads)
-    barrier = pltpu.get_barrier_semaphore()
-    far_first(lambda dz, dx: pl.semaphore_signal(
-        barrier, inc=1, device_id=(at_offset(dz, dx), mt), device_id_type=MESH))
-    for d in away[::-1]:
-        for c in range(CORES):
-            pl.semaphore_signal(
-                barrier, inc=1, device_id=(me, chip(d) * CORES + c), device_id_type=MESH)
-    pl.semaphore_signal(barrier, inc=1, device_id=(me, twin), device_id_type=MESH)
 
     mark("local_copies")
     own_cols = pl.ds(pl.multiple_of(mt * d_local, d_local), d_local)
@@ -188,45 +189,51 @@
         shift *= 2
     lane = iota((states, tok), 1)
     bypass = byp_ref[...]
-    for g in range(groups):
-        row = slice(g, g + 1)
-        u = u_ref[g * lanes:(g + 1) * lanes, :].astype(F32)
-        e_re = dot_first(ein_ref[g], u)
-        e_im = dot_first(eq_ref[g], u)
-        f_re, f_im = to_col(fac_re[row]), to_col(fac_im[row])
-        s_re, s_im = times(f_re, f_im, e_re, e_im)
-        rate_c = to_col(rate[row])
-        w_re, w_im = to_col(cos[row]), to_col(sin[row])
-        sums = total[row]
-        p_re, p_im = jnp.ones((states, tok), F32), jnp.zeros((states, tok), F32)
+    each_group = range(groups)
+    rows_g = [slice(g, g + 1) for g in each_group]
+    signal = [u_ref[g * lanes:(g + 1) * lanes, :].astype(F32) for g in each_group]
+    e_re = [dot_first(ein_ref[g], signal[g]) for g in each_group]
+    e_im = [dot_first(eq_ref[g], signal[g]) for g in each_group]
+    rate_c = [to_col(rate[row]) for row in rows_g]
+    w = [(to_col(cos[row]), to_col(sin[row])) for row in rows_g]
+    s = [
+        times(to_col(fac_re[row]), to_col(fac_im[row]), e_re[g], e_im[g])
+        for g, row in enumerate(rows_g)]
+    p = [(jnp.ones((states, tok), F32), jnp.zeros((states, tok), F32))] * groups
+    for pair in GROUP_SETS:
         shift = 1
         while shift <= tok:
             taken = (jnp.bitwise_and(lane + 1, shift)) != 0
-            q_re, q_im = times(p_re, p_im, w_re, w_im)
-            p_re, p_im = jnp.where(taken, q_re, p_re), jnp.where(taken, q_im, p_im)
-            if shift < tok:
-                gap = sums - pltpu.roll(sums, shift, 1)
-                size = jnp.exp(rate_c * float(shift) + jnp.minimum(gap, 0.0))
-                size = jnp.where(lane >= shift, size, 0.0)
-                t_re, t_im = times(
-                    w_re, w_im, pltpu.roll(s_re, shift, 1), pltpu.roll(s_im, shift, 1))
-                s_re, s_im = s_re + size * t_re, s_im + size * t_im
-                w_re, w_im = times(w_re, w_im, w_re, w_im)
+            for g in pair:
+                sums = total[rows_g[g]]
+                q_re, q_im = times(*p[g], *w[g])
+                p[g] = jnp.where(taken, q_re, p[g][0]), jnp.where(taken, q_im, p[g][1])
+                if shift < tok:
+                    gap = sums - pltpu.roll(sums, shift, 1)
+                    size = jnp.exp(rate_c[g] * float(shift) + jnp.minimum(gap, 0.0))
+                    size = jnp.where(lane >= shift, size, 0.0)
+                    t_re, t_im = times(
+                        *w[g], pltpu.roll(s[g][0], shift, 1), pltpu.roll(s[g][1], shift, 1))
+                    s[g] = s[g][0] + size * t_re, s[g][1] + size * t_im
+                    w[g] = times(*w[g], *w[g])
             shift *= 2
-        size = jnp.exp(rate_c * (lane + 1).astype(F32) + sums)
-        cum_r[g], cum_i[g] = size * p_re, size * p_im
-        last = lane == tok - 1
-        h_re = to_row(jnp.sum(jnp.where(last, s_re, 0.0), axis=1, keepdims=True))
-        h_im = to_row(jnp.sum(jnp.where(last, s_im, 0.0), axis=1, keepdims=True))
-        end = jnp.sum(jnp.where(lane_g[row] == tok - 1, sums, 0.0), axis=1, keepdims=True)
+        for g in pair:
+            size = jnp.exp(rate_c[g] * (lane + 1).astype(F32) + total[rows_g[g]])
+            cum_r[g], cum_i[g] = size * p[g][0], size * p[g][1]
+    last = lane == tok - 1
+    for g, row in enumerate(rows_g):
+        h_re = to_row(jnp.sum(jnp.where(last, s[g][0], 0.0), axis=1, keepdims=True))
+        h_im = to_row(jnp.sum(jnp.where(last, s[g][1], 0.0), axis=1, keepdims=True))
+        end = jnp.sum(
+            jnp.where(lane_g[row] == tok - 1, total[row], 0.0), axis=1, keepdims=True)
         msg[g:g + 1, 0:states] = h_re
         msg[g:g + 1, states:2 * states] = jnp.broadcast_to(end, (1, states))
         msg[groups + g:groups + g + 1, 0:states] = h_im
         msg[groups + g:groups + g + 1, states:2 * states] = jnp.zeros((1, states), F32)
         loc_r[g] = (
-            jnp.dot(cin_ref[g], s_re, precision=HIGH, preferred_element_type=F32)
-            - jnp.dot(cq_ref[g], s_im, precision=HIGH, preferred_element_type=F32)
-            + to_col(bypass[:, g * lanes:(g + 1) * lanes]) * u)
+            jnp.dot(cin_ref[g], s[g][0], precision=HIGH, preferred_element_type=F32)
+            - jnp.dot(cq_ref[g], s[g][1], precision=HIGH, preferred_element_type=F32)
+            + to_col(bypass[:, g * lanes:(g + 1) * lanes]) * signal[g])
 
     mark("barrier")
     pl.semaphore_wait(barrier, n_sp - 1 + n_tp - 1)
@@ -342,7 +349,7 @@
     mark("wait_quarter")
     local[2].wait()
     each(n_tp, mt, lambda k: got(wx.at[k, quarter, :], r_wx.at[k]))
-    for j in range(1, X_CHIPS):
+    for j in (2, 1, 3):
         send_quarter(j).start()
     send_dw_to(targets[DW_EARLY:DW_MID])
     send_dw(twin).start()
@@ -645,7 +652,7 @@
     ]
     return pl.pallas_call(
         functools.partial(mixer_kernel, dims),
-        out_shape=jax.ShapeDtypeStruct((tok, d_local), BF16),
+        out_shape=pltpu.VMEM((tok, d_local), BF16),
         in_specs=[hbm] * 18,
         out_specs=vmem,
         scratch_shapes=scratch,

time: 96.6 us -> 94.8 us (0.981)
  no operation moved by 1% of the time
where the time goes in v4:
time: 94.8 us; the launch traced here: 94.6 us
  Pallas kernels  94 us (99%)
    pallas_call x1, Pallas kernels, per_device(): pl.pallas_call(functools.partial(mixer_kernel, dims), out_shape=pltpu.VME...  94 us

profile of v4, /device:TPU:1, one launch (start us, length us, event | category | flops | bytes accessed | tf_op | source)
XLA Modules:
  0.0 94.6 jit_solution(4064521574990935378)
XLA Ops:
  0.0 94.0 %shard_map.172 = bf16[128,256]{1,0:T(8,128)(2,1)S(1)} custom-call(bf16[64,128]{1,0:T(8,128)(2,1)} %u_hbm.1, f32[4,64]{1,0:T(4,128)} %damp_hbm.1, f32[4,64]{1,0:T(4,128)} %ang_hbm.1, f32[1,4]{1,0:T(1,128)} %bitcast.12, f32[4,16,64]{2,1,0:T(8,128)} %bitcast.7, f32[4,16,64]{2,1,0:T(8,128)} %bitcast.8, f32[4,16,64]{2,1,0:T(8,128)} %cin_hbm.1, ...), custom_call_target="tpu_custom_call" | custom-call | tf_op jit(solution)/shard_map/pallas_call | solution.py:653
  94.0 0.6 copy.20

commit v5 on v4

--- a/solution.py
+++ b/solution.py
@@ -14,7 +14,7 @@
 BF16 = jnp.bfloat16
 CORES = 2
 CHUNKS = 4
-SKEW = 0.5
+SKEW = 0.4
 X_CHIPS = 4
 DW_EARLY, DW_MID = 4, 12
 PIECE = 32

time: 94.8 us -> 93.7 us (0.988)
  Pallas kernels: 94 us -> 92.9 us
    pallas_call x1, Pallas kernels: 94 us -> 92.9 us  [per_device(): pl.pallas_call(functools.partial(mixer_kernel, dims), out_shape=pltpu.VME...]
where the time goes in v5:
time: 93.7 us; the launch traced here: 93.6 us
  Pallas kernels  92.9 us (99%)
    pallas_call x1, Pallas kernels, per_device(): pl.pallas_call(functools.partial(mixer_kernel, dims), out_shape=pltpu.VME...  92.9 us

profile of v5, /device:TPU:1, one launch (start us, length us, event | category | flops | bytes accessed | tf_op | source)
XLA Modules:
  0.0 93.6 jit_solution(9769882138772192506)
XLA Ops:
  0.0 92.9 %shard_map.172 = bf16[128,256]{1,0:T(8,128)(2,1)S(1)} custom-call(bf16[64,128]{1,0:T(8,128)(2,1)} %u_hbm.1, f32[4,64]{1,0:T(4,128)} %damp_hbm.1, f32[4,64]{1,0:T(4,128)} %ang_hbm.1, f32[1,4]{1,0:T(1,128)} %bitcast.12, f32[4,16,64]{2,1,0:T(8,128)} %bitcast.7, f32[4,16,64]{2,1,0:T(8,128)} %bitcast.8, f32[4,16,64]{2,1,0:T(8,128)} %cin_hbm.1, ...), custom_call_target="tpu_custom_call" | custom-call | tf_op jit(solution)/shard_map/pallas_call | solution.py:653
  93.0 0.6 copy.20
